TPU v7x, 32 devices: a whole 2x2x4 slice. The times are simulated.
32 devices in a mesh: ep: 4 (over y, x), tp: 8 (over z, core).
Axes of the slice: x: 2, y: 2, z: 4, core: 2. Of those that a mesh axis runs over, the one named last changes fastest.
Arguments:
- mixer_in: bfloat16 [8192, 2048], P(('ep', 'tp')), may hold values from -6 to 6
- pre_gain: float32 [2048], replicated, may hold values from 0.1 to 1.9
- glu_value: bfloat16 [2048, 1024], P(None, 'tp'), may hold values from -0.125 to 0.125
- glu_gate: bfloat16 [2048, 1024], P(None, 'tp'), may hold values from -0.125 to 0.125
- conv_kernel: float32 [31, 1024], replicated, may hold values from -1 to 1
- chan_gain: float32 [1024], replicated, may hold values from 0.1 to 1.9
- out_weight: bfloat16 [1024, 2048], P(None, 'tp'), may hold values from -0.1875 to 0.1875
- mix_gain: float32 [2048], replicated, may hold values from 0.1 to 1.9
- expert_in: bfloat16 [1024, 2048], P(('ep', 'tp')), may hold values from -6 to 6
- ffn_gain: float32 [2048], replicated, may hold values from 0.1 to 1.9
- routing: int32 [1024, 2], P(('ep', 'tp')), may hold values from 0 to 7, all different within a row; in each aligned block of 32 rows (0 to 31, 32 to 63, ...) at most 12 rows name the same one
- route_weight: float32 [1024, 2], P(('ep', 'tp')), may hold values from 0.1 to 1
- gate_proj: bfloat16 [8, 2048, 4096], P('ep', None, 'tp'), may hold values from -0.375 to 0.375
- up_proj: bfloat16 [8, 2048, 4096], P('ep', None, 'tp'), may hold values from -0.375 to 0.375
- down_proj: bfloat16 [8, 4096, 2048], P('ep', 'tp'), may hold values from -0.09375 to 0.09375
- expert_gain: float32 [2048], replicated, may hold values from 0.1 to 1.9
Outputs:
- mixed: bfloat16 [8192, 2048], P(('ep', 'tp'))
- routed: bfloat16 [1024, 2048], P(('ep', 'tp'))
Inputs may be any that keep to these rules, and one draw needn't show every extreme that they name: `routing`: each row names 2 different experts; in each aligned block of 32 rows (the rows of one device) no expert is named more than 12 times.
All inputs are finite; a program needn't handle non-finite values.
Results may differ from a plain program's by a relative error of at most 0.02.
Values may be sent and summed in bfloat16 or wider, within the bound.
No kernel may reach another device: no remote copies, remote signals or barrier semaphores. Data moves between devices by JAX's collectives and lax.ppermute only.
A program may use at most 128 MiB of HBM per device.

v0:
```python
import jax
import jax.numpy as jnp
from jax import lax
from jax.sharding import PartitionSpec as P

RMS_EPSILON = 1e-06
LAYER_EPSILON = 1e-05
CLAMP_LIMIT = 7.0
SWISH_ALPHA = 1.702


def passed_along(value, axis, steps):
    count = lax.axis_size(axis)
    initial, last = (max(0, -steps), min(count, count - steps))
    return lax.ppermute(value, axis, [(source, source + steps) for source in range(initial, last)])


def rms_scale(values, gain_row):
    values = values.astype(jnp.float32)
    return (
        values
        * lax.rsqrt(jnp.mean(values * values, axis=-1, keepdims=True) + RMS_EPSILON)
        * gain_row
    )


def on_device(
    mixer_in,
    pre_gain,
    glu_value,
    glu_gate,
    conv_kernel,
    chan_gain,
    out_weight,
    mix_gain,
    expert_in,
    ffn_gain,
    routing,
    route_weight,
    gate_proj,
    up_proj,
    down_proj,
    expert_gain,
):
    groups_ep = lax.axis_size("ep")
    local_experts = gate_proj.shape[0]
    experts = local_experts * groups_ep
    token_rows, top_count = routing.shape
    capacity = max(2, 3 * token_rows * top_count // (2 * experts))
    flat_route = routing.reshape(-1)
    onehot = (flat_route[:, None] == jnp.arange(experts, dtype=jnp.int32)[None, :]).astype(
        jnp.int32
    )
    before = jnp.cumsum(onehot, axis=0) - onehot
    rank_within = jnp.sum(before * onehot, axis=1)
    slot_index = (flat_route * capacity + rank_within).reshape(token_rows, top_count)
    slot_ids = jnp.arange(experts * capacity, dtype=jnp.int32)
    chosen = slot_index[None, :, :] == slot_ids[:, None, None]
    pick_matrix = jnp.sum(chosen.astype(jnp.float32), axis=2).astype(jnp.bfloat16)
    normed_exp = rms_scale(expert_in, ffn_gain).astype(jnp.bfloat16)
    outgoing = jnp.dot(pick_matrix, normed_exp, preferred_element_type=jnp.float32).astype(
        jnp.bfloat16
    )
    outgoing = outgoing.reshape(groups_ep, local_experts * capacity, outgoing.shape[1])
    arrived = lax.all_to_all(outgoing, "ep", split_axis=0, concat_axis=0, tiled=True)
    value_full, gate_full, out_full, every_row = (
        lax.all_gather(glu_value, "tp", axis=1, tiled=True),
        lax.all_gather(glu_gate, "tp", axis=1, tiled=True),
        lax.all_gather(out_weight, "tp", axis=1, tiled=True),
        lax.all_gather(arrived, "tp", axis=0, tiled=True),
    )
    row_block = every_row.reshape(every_row.shape[0], local_experts, capacity, every_row.shape[2])
    gate_pre = jnp.einsum(
        "xecd,edf->xecf", row_block, gate_proj, preferred_element_type=jnp.float32
    )
    up_pre = jnp.einsum("xecd,edf->xecf", row_block, up_proj, preferred_element_type=jnp.float32)
    gate_pre = jnp.minimum(gate_pre, CLAMP_LIMIT)
    up_pre = jnp.clip(up_pre, -CLAMP_LIMIT, CLAMP_LIMIT)
    hidden_act = ((up_pre + 1.0) * gate_pre * jax.nn.sigmoid(SWISH_ALPHA * gate_pre)).astype(
        jnp.bfloat16
    )
    normed_mix = rms_scale(mixer_in, pre_gain).astype(jnp.bfloat16)
    value_pre = jnp.dot(normed_mix, value_full, preferred_element_type=jnp.float32)
    gate_mix = jnp.dot(normed_mix, gate_full, preferred_element_type=jnp.float32)
    gated_rows = (value_pre * jax.nn.sigmoid(gate_mix)).astype(jnp.bfloat16)
    kernel_width = conv_kernel.shape[0]
    length = gated_rows.shape[0]
    rim_rows = passed_along(gated_rows[length - (kernel_width - 1) :], ("ep", "tp"), 1)
    padded = jnp.concatenate([rim_rows, gated_rows], axis=0).astype(jnp.float32)
    conv_sum = jnp.zeros((length, gated_rows.shape[1]), jnp.float32)
    for offset in range(kernel_width):
        conv_sum = conv_sum + conv_kernel[offset] * padded[offset : offset + length]
    row_mean = jnp.mean(conv_sum, axis=-1, keepdims=True)
    centred = conv_sum - row_mean
    row_var = jnp.mean(centred * centred, axis=-1, keepdims=True)
    activated = jax.nn.silu(centred * lax.rsqrt(row_var + LAYER_EPSILON) * chan_gain).astype(
        jnp.bfloat16
    )
    projected = jnp.dot(activated, out_full, preferred_element_type=jnp.float32)
    mixed = rms_scale(projected, mix_gain).astype(jnp.bfloat16)
    summed = lax.psum_scatter(
        jnp.einsum(
            "xecf,efd->xecd", hidden_act, down_proj, preferred_element_type=jnp.float32
        ).astype(jnp.bfloat16),
        "tp",
        scatter_dimension=0,
        tiled=True,
    )
    returned = lax.all_to_all(summed, "ep", split_axis=0, concat_axis=0, tiled=True)
    returned = returned.reshape(experts * capacity, returned.shape[3])
    combined = jnp.zeros((token_rows, returned.shape[1]), jnp.float32)
    for column in range(top_count):
        combined = combined + route_weight[:, column][:, None] * returned[
            slot_index[:, column]
        ].astype(jnp.float32)
    routed = rms_scale(combined, expert_gain).astype(jnp.bfloat16)
    return (mixed, routed)


def solution(mesh):
    in_specs = (
        P(("ep", "tp"), None),
        P(),
        P(None, "tp"),
        P(None, "tp"),
        P(),
        P(),
        P(None, "tp"),
        P(),
        P(("ep", "tp"), None),
        P(),
        P(("ep", "tp"), None),
        P(("ep", "tp"), None),
        P("ep", None, "tp"),
        P("ep", None, "tp"),
        P("ep", "tp", None),
        P(),
    )
    out_specs = (P(("ep", "tp"), None), P(("ep", "tp"), None))
    return jax.shard_map(
        on_device, mesh=mesh, in_specs=in_specs, out_specs=out_specs, check_vma=False
    )
```

profile of v0, /device:TPU:0, one launch (start us, length us, event | category | flops | bytes accessed | tf_op | source)
XLA Modules:
  0.0 298.7 jit_solution(17290672283870589739)
XLA Ops:
  7.2 0.0 all-gather.11.cloned.1.call-start
  7.2 0.8 copy.45
  8.0 0.1 eq.28
  8.1 0.1 fusion.73
  8.2 0.1 reduce_window_sum.11
  8.3 0.2 select_reduce_fusion
  8.4 0.1 reduce_sum.79
  8.5 0.1 copy.46
  8.6 0.7 multiply_add_fusion.1
  9.3 0.1 convert_reduce_fusion
  9.4 1.0 fusion.67
  10.5 1.2 convolution_convert_fusion
  11.7 12.2 %all_to_all.10 = bf16[4,24,2048]{2,1,0:T(8,128)(2,1)} all-to-all(bf16[4,24,2048]{2,1,0:T(8,128)(2,1)S(1)} %bitcast.81), channel_id=1, replica_groups=mesh['ep'=4,'tp'=8] {'ep'}, dimensions={0} | all-to-all | bytes 786432 | tf_op jit(solution)/shard_map/all_to_all | solution.py:65
  23.9 0.0 all-gather.11.cloned.1.call-update
  23.9 0.0 all-gather.7.cloned.1.call-start
  24.0 0.7 all-gather.7.cloned.1.call-update
  24.7 0.0 all-gather.5.cloned.1.call-start
  24.7 0.7 all-gather.5.cloned.1.call-update
  25.4 0.0 all-reduce.3.cloned.1.call-start
  25.5 36.6 %all-gather.11.cloned.1.call-done = bf16[32,24,2048]{2,1,0:T(8,128)(2,1)} async-done(((bf16[4,24,2048]{2,1,0:T(8,128)(2,1)}), bf16[32,24,2048]{2,1,0:T(8,128)(2,1)}) %all-gather.11.cloned.1.call-update) | async-done | bytes 3145744 | tf_op jit(solution)/shard_map/all_gather | solution.py:70
  62.0 3.8 %copy.47 = bf16[32,24,2048]{2,0,1:T(8,128)(2,1)S(1)} copy(bf16[32,24,2048]{2,1,0:T(8,128)(2,1)} %all-gather.11.cloned.1.call-done) | data formatting | bytes 6291456 | tf_op jit(solution)/shard_map/all_gather | solution.py:70
  65.8 0.0 copy-done.5
  65.8 3.0 %fusion.2 = f32[2,32,12,512]{3,1,2,0:T(8,128)} fusion(bf16[32,2,12,2048]{3,0,2,1:T(8,128)(2,1)S(1)} %bitcast.79, bf16[2,2048,512]{2,1,0:T(8,128)(2,1)S(1)} %copy-done.5), kind=kOutput, calls=%fused_computation.4 | convolution fusion | flops 1610612736 | bytes 8912896 | tf_op jit(solution)/shard_map/xecd,edf->xecf/dot_general | solution.py:73
  68.8 9.8 %fusion.9 = bf16[32,2,12,2048]{3,0,2,1:T(8,128)(2,1)} fusion(bf16[2,512,2048]{2,1,0:T(8,128)(2,1)} %param.30, f32[2,32,12,512]{3,1,2,0:T(8,128)} %fusion.2, bf16[32,2,12,2048]{3,0,2,1:T(8,128)(2,1)S(1)} %bitcast.80, bf16[2,2048,512]{2,1,0:T(8,128)(2,1)} %param.29), kind=kOutput, calls=%fused_computation.9 | convolution fusion | flops 3226730496 | bytes 16252928 | tf_op jit(solution)/shard_map/xecf,efd->xecd/dot_general | solution.py:102
  78.6 0.0 copy-start.6
  78.6 0.0 all-reduce.3.cloned.1.call-update
  78.7 0.0 all-gather.9.cloned.1.call-start
  78.7 0.5 all-gather.9.cloned.1.call-update
  79.2 0.0 copy-done.8
  79.3 0.6 dynamic-slice
  80.5 0.0 copy-done
  80.5 0.3 fusion.12
  80.8 0.0 copy-done.4
  80.9 0.0 copy-done.1
  80.9 0.1 fusion.84
  81.0 29.4 %all-gather.7.cloned.1.call-done = bf16[2048,1024]{1,0:T(8,128)(2,1)} async-done(((bf16[2048,128]{1,0:T(8,128)(2,1)}), bf16[2048,1024]{1,0:T(8,128)(2,1)}) %all-gather.7.cloned.1.call-update) | async-done | bytes 4194320 | tf_op jit(solution)/shard_map/all_gather | solution.py:68
  110.4 0.0 copy-done.6
  110.4 3.6 %fusion.19 = f32[256,1024]{1,0:T(8,128)S(1)} fusion(bf16[2048,1024]{1,0:T(8,128)(2,1)} %all-gather.7.cloned.1.call-done, bf16[256,2048]{1,0:T(8,128)(2,1)S(1)} %copy-done, f32[2048]{0:T(1024)S(1)} %copy-done.6, f32[256]{0:T(256)S(1)} %add_rsqrt_fusion.2), kind=kOutput, calls=%fused_computation.23 | convolution fusion | flops 1076625408 | bytes 6300672 | tf_op jit(solution)/shard_map/dot_general | solution.py:84
  113.9 44.1 %all-gather.5.cloned.1.call-done = bf16[2048,1024]{1,0:T(8,128)(2,1)} async-done(((bf16[2048,128]{1,0:T(8,128)(2,1)}), bf16[2048,1024]{1,0:T(8,128)(2,1)}) %all-gather.5.cloned.1.call-update) | async-done | bytes 4194320 | tf_op jit(solution)/shard_map/all_gather | solution.py:67
  158.0 3.5 %fusion.20 = bf16[256,1024]{1,0:T(8,128)(2,1)S(1)} fusion(f32[256,1024]{1,0:T(8,128)S(1)} %fusion.19, bf16[2048,1024]{1,0:T(8,128)(2,1)} %all-gather.5.cloned.1.call-done, bf16[256,2048]{1,0:T(8,128)(2,1)S(1)} %copy-done, f32[2048]{0:T(1024)S(1)} %copy-done.6, f32[256]{0:T(256)S(1)} %add_rsqrt_fusion.2), kind=kOutput, calls=%fused_computation.24 | convolution fusion | flops 1076363264 | bytes 6824960 | tf_op jit(solution)/shard_map/dot_general | solution.py:83
  161.6 2.2 collective-permute-start
  163.7 71.6 %all-reduce.3.cloned.1.call-done = bf16[32,2,12,2048]{3,0,2,1:T(8,128)(2,1)} async-done(((bf16[32,2,12,2048]{3,0,2,1:T(8,128)(2,1)}), bf16[32,2,12,2048]{3,0,2,1:T(8,128)(2,1)}) %all-reduce.3.cloned.1.call-update) | async-done | bytes 3145744
  235.3 1.4 constant_dynamic-slice_fusion
  236.7 1.2 copy.48
  237.8 3.6 %all-to-all-start.1 = ((bf16[4,2,12,2048]{3,1,2,0:T(2,128)(2,1)}), bf16[4,2,12,2048]{3,1,2,0:T(2,128)(2,1)S(1)}, u32[]{:S(2)}, u32[]{:S(2)}) async-start(bf16[4,2,12,2048]{3,1,2,0:T(2,128)(2,1)} %copy.48), calls=%async_computation.1 | async-start | bytes 786432 | tf_op jit(solution)/shard_map/all_to_all | solution.py:109
  241.5 0.0 collective-permute-done
  241.5 0.1 maximum_convert_fusion
  241.6 0.0 copy-start.7
  241.6 5.4 %fusion.82 = (f32[256]{0:T(256)S(1)}, f32[256,1024]{1,0:T(8,128)S(1)}) fusion(f32[286,1024]{1,0:T(8,128)S(1)} %maximum_convert_fusion, f32[1024]{0:T(1024)S(1)} %bitcast.92, f32[1024]{0:T(1024)S(1)} %bitcast.93, f32[1024]{0:T(1024)S(1)} %bitcast.95, f32[1024]{0:T(1024)S(1)} %bitcast.96, f32[1024]{0:T(1024)S(1)} %bitcast.97, f32[1024]{0:T(1024)S(1)} %bitcast.98, ...), kind=kLoop, calls=%fused_computation.136 | loop fusion | flops 16252672 | bytes 33682432 | tf_op jit(solution)/shard_map/reduce_sum | solution.py:93
  247.1 0.2 multiply_reduce_fusion.1
  247.4 0.0 copy-start.2
  247.4 37.1 %all-gather.9.cloned.1.call-done = bf16[1024,2048]{1,0:T(8,128)(2,1)} async-done(((bf16[1024,256]{1,0:T(8,128)(2,1)}), bf16[1024,2048]{1,0:T(8,128)(2,1)}) %all-gather.9.cloned.1.call-update) | async-done | bytes 4194320 | tf_op jit(solution)/shard_map/all_gather | solution.py:69
  284.5 0.0 copy-done.7
  284.5 3.8 %multiply_reduce_fusion = (f32[256]{0:T(256)S(1)}, f32[256,2048]{1,0:T(8,128)S(1)}) fusion(bf16[1024,2048]{1,0:T(8,128)(2,1)} %all-gather.9.cloned.1.call-done, f32[256,1024]{1,0:T(8,128)S(1)} %get-tuple-element.3, f32[1024]{0:T(1024)S(1)} %copy-done.7, f32[256]{0:T(256)S(1)} %add_rsqrt_fusion.1, f32[256]{0:T(256)S(1)} %broadcast_multiply_fusion), kind=kOutput, calls=%fused_computation.17 | convolution fusion | flops 1076887296 | bytes 7347200 | tf_op jit(solution)/shard_map/dot_general | solution.py:99
  288.3 0.0 copy-done.2
  288.3 1.2 multiply_convert_fusion
  289.5 0.0 all-to-all-done.1
  289.5 0.1 copy.49
  289.7 0.1 reshape.74
  289.8 0.7 gather_fusion
  290.4 0.7 gather_fusion.1
  291.1 0.2 multiply_reduce_fusion.2
  291.3 0.0 copy-done.3
  291.4 0.8 multiply_convert_fusion.4
  (17 shorter events, 0.1 us)
Async XLA Ops:
  7.2 54.9 %all-gather.11.cloned.1.call-start = ((), (), s32[]{:S(2)}) async-start(), calls=%async_computation.5 | async-start | bytes 3538944 | tf_op jit(solution)/shard_map/all_gather | solution.py:70
  23.9 86.4 %all-gather.7.cloned.1.call-start = ((), (), s32[]{:S(2)}) async-start(), calls=%async_computation.3 | async-start | bytes 4718592 | tf_op jit(solution)/shard_map/all_gather | solution.py:68
  24.7 133.3 %all-gather.5.cloned.1.call-start = ((), (), s32[]{:S(2)}) async-start(), calls=%async_computation.2 | async-start | bytes 4718592 | tf_op jit(solution)/shard_map/all_gather | solution.py:67
  25.4 209.9 %all-reduce.3.cloned.1.call-start = ((), (), s32[]{:S(2)}) async-start(), calls=%async_computation.6 | async-start | bytes 6291456
  62.0 3.8 %copy-start.5 = (bf16[2,2048,512]{2,1,0:T(8,128)(2,1)S(1)}, bf16[2,2048,512]{2,1,0:T(8,128)(2,1)}, u32[]{:S(2)}) copy-start(bf16[2,2048,512]{2,1,0:T(8,128)(2,1)} %param.28) | copy-start | bytes 12582916
  78.6 0.7 copy-start.8
  78.6 1.9 copy-start
  78.6 2.2 copy-start.4
  78.6 2.2 copy-start.1
  78.6 31.7 %copy-start.6 = (f32[2048]{0:T(1024)S(1)}, f32[2048]{0:T(1024)}, u32[]{:S(2)}) copy-start(f32[2048]{0:T(1024)} %param.17) | copy-start | bytes 24580
  78.7 205.8 %all-gather.9.cloned.1.call-start = ((), (), s32[]{:S(2)}) async-start(), calls=%async_computation.4 | async-start | bytes 4718592 | tf_op jit(solution)/shard_map/all_gather | solution.py:69
  161.6 79.9 %collective-permute-start = (bf16[30,1024]{1,0:T(8,128)(2,1)S(1)}, bf16[30,1024]{1,0:T(8,128)(2,1)S(1)}, u32[]{:S(2)}, u32[]{:S(2)}) collective-permute-start(bf16[30,1024]{1,0:T(8,128)(2,1)S(1)} %slice.272), channel_id=1, source_target_pairs={{0,1},{1,2},{2,3},{3,4},{4,5},{5,6},{6,7},{7,8},{8,9},{9,10},{10,1... | collective-permute-start | bytes 184328 | tf_op jit(solution)/shard_map/ppermute | solution.py:15
  237.8 51.7 %all-to-all-start.1 = ((bf16[4,2,12,2048]{3,1,2,0:T(2,128)(2,1)}), bf16[4,2,12,2048]{3,1,2,0:T(2,128)(2,1)S(1)}, u32[]{:S(2)}, u32[]{:S(2)}) async-start(bf16[4,2,12,2048]{3,1,2,0:T(2,128)(2,1)} %copy.48), calls=%async_computation.1 | async-start | bytes 786432 | tf_op jit(solution)/shard_map/all_to_all | solution.py:109
  241.6 42.9 %copy-start.7 = (f32[1024]{0:T(1024)S(1)}, f32[1024]{0:T(1024)}, u32[]{:S(2)}) copy-start(f32[1024]{0:T(1024)} %param.21) | copy-start | bytes 12292
  247.4 40.9 %copy-start.2 = (f32[2048]{0:T(1024)S(1)}, f32[2048]{0:T(1024)}, u32[]{:S(2)}) copy-start(f32[2048]{0:T(1024)} %param.23) | copy-start | bytes 24580
  289.5 1.8 copy-start.3
Sparse Core Ops, SparseCore 0:
  24.0 37.9 all-gather.10
  63.6 46.7 all-gather.6
  112.0 45.9 all-gather.4
  160.2 75.0 all-reduce.2
  236.7 47.7 all-gather.8
where the time goes:
time: 299 us
  waiting for transfers between devices  221 us (74%)
  matrix products  24.9 us (8%)
  between operations  14.7 us (5%)
  blocking collectives  12.2 us (4%)
  other arithmetic  10.6 us (4%)
  local copies, waits for them, and re-layouts  9.62 us (3%)
  starting transfers between devices  6.01 us (2%)
    unnamed x6, waiting for transfers between devices  73.5 us
    all_gather x1, waiting for transfers between devices, on_device(): lax.all_gather(glu_value, 'tp', axis=1, tiled=True)  44.1 us
    all_gather x1, waiting for transfers between devices, on_device(): lax.all_gather(out_weight, 'tp', axis=1, tiled=True)  37.1 us
    all_gather x1, waiting for transfers between devices, on_device(): lax.all_gather(arrived, 'tp', axis=0, tiled=True)  36.6 us
    all_gather x1, waiting for transfers between devices, on_device(): lax.all_gather(glu_gate, 'tp', axis=1, tiled=True)  29.4 us
    all_to_all x1, blocking collectives, on_device(): lax.all_to_all(outgoing, 'ep', split_axis=0, concat_axis=0, tiled=True)  12.2 us
    dot_general x1, matrix products, on_device(): jnp.einsum('xecf,efd->xecd', hidden_act, down_proj, preferred_element_typ...  9.8 us
  transfers between devices with their start and end apart: 7, of which 5 were waited for; matrix products, arithmetic and copies ran while one was open for 13% of the time, Pallas kernels for 0%

commit v1 on v0

v1 whole, which is shorter than its diff:
```python
import functools

import jax
import jax.numpy as jnp
from jax import lax
from jax.experimental import pallas as pl
from jax.experimental.pallas import tpu as pltpu
from jax.sharding import PartitionSpec as P


RMS_EPSILON = 1e-06
LAYER_EPSILON = 1e-05
CLAMP_LIMIT = 7.0
SWISH_ALPHA = 1.702
SPARE_VMEM = 6 * 1024 * 1024


def passed_along(value, axis, steps):
    count = lax.axis_size(axis)
    initial, last = (max(0, -steps), min(count, count - steps))
    return lax.ppermute(value, axis, [(source, source + steps) for source in range(initial, last)])


def swapped(value, ep_bits, tp_bits):
    count_ep, count_tp = lax.axis_size("ep"), lax.axis_size("tp")
    pairs = [
        (e * count_tp + t, (e ^ ep_bits) * count_tp + (t ^ tp_bits))
        for e in range(count_ep)
        for t in range(count_tp)
    ]
    return lax.ppermute(value, ("ep", "tp"), pairs)


def column_shared(value):
    return [swapped(value, 0, 2 * bits) for bits in range(1, lax.axis_size("tp") // 2)]


def plane_shared(value, axis):
    count_ep = lax.axis_size("ep")
    if count_ep != 4:
        return [[swapped(value, bits, 0)] for bits in range(1, count_ep)]
    half = value.shape[axis] // 2
    near = [swapped(value, 1, 0), swapped(value, 2, 0)]
    low = swapped(lax.slice_in_dim(near[0], 0, half, axis=axis), 2, 0)
    high = swapped(lax.slice_in_dim(near[1], half, 2 * half, axis=axis), 1, 0)
    return [[near[0]], [near[1]], [low, high]]


def rms_scale(values, gain_row):
    values = values.astype(jnp.float32)
    return (
        values
        * lax.rsqrt(jnp.mean(values * values, axis=-1, keepdims=True) + RMS_EPSILON)
        * gain_row
    )


def weights_body(places, value_ref, gate_ref, out_ref, glu_ref, glu_part_ref, out_part_ref):
    channels = value_ref.shape[1]
    glu_ref[:, :channels] = value_ref[...]
    glu_ref[:, channels:] = gate_ref[...]
    for full, part in ((value_ref, glu_part_ref), (gate_ref, glu_part_ref), (out_ref, out_part_ref)):
        depth = part.shape[0]
        start = pl.multiple_of(places[0] * depth, depth)
        rows = full[pl.ds(start, depth), :]
        if full is gate_ref:
            part[:, channels:] = rows
        else:
            part[:, : full.shape[1]] = rows


def gathered_blocks(own, mine):
    column = packed(column_shared(mine))
    pieces = [[column]] + plane_shared(column, 1)
    other = [[swapped(part, 0, 1) for part in parts] for parts in pieces]
    return (own, pieces), (swapped(own, 0, 1), other)


def flat_refs(weight_sets):
    return [
        part for own, pieces in weight_sets for part in [own] + [p for parts in pieces for p in parts]
    ]


def unflat_refs(refs, counts):
    sets, at = [], 0
    for _ in range(2):
        own, pieces = refs[at], []
        at += 1
        for count in counts:
            pieces.append(refs[at : at + count])
            at += count
        sets.append((own, pieces))
    return sets


def block_products(rows_ref, places, own_ref, pieces, quarter, block):
    total = None
    for bits, parts in enumerate(pieces):
        if block == 0:
            terms = [(0, quarter, own_ref[bits * quarter : (bits + 1) * quarter, :])]
        else:
            terms, at = [], 0
            for part in parts:
                terms.append((at, part.shape[1], part[block - 1]))
                at += part.shape[1]
        columns = bits if block == 0 else places[0] ^ bits
        for at, depth, weight in terms:
            if len(rows_ref.shape) == 3:
                rows = rows_ref[columns][:, at : at + depth]
            else:
                rows = rows_ref[:, pl.ds(pl.multiple_of(columns * quarter, quarter) + at, depth)]
            term = jnp.dot(rows, weight, preferred_element_type=jnp.float32)
            total = term if total is None else total + term
    return total


def by_quarter(rows, count):
    length, depth = rows.shape
    if (depth // count) % 128 == 0:
        return rows
    return rows.reshape(length, count, depth // count).transpose(1, 0, 2)


def glu_body(counts, places, rows_ref, *refs):
    glu_ref, rim_ref = refs[-2], refs[-1]
    channels = glu_ref.shape[2]
    quarter = refs[0].shape[0] // len(counts)
    for core, (own_ref, pieces) in enumerate(unflat_refs(refs, counts)):
        for block in range(glu_ref.shape[0] // 2):
            pre = block_products(rows_ref, places, own_ref, pieces, quarter, block)
            out = pre[:, :channels] * jax.nn.sigmoid(pre[:, channels:])
            out = out.astype(glu_ref.dtype)
            glu_ref[places[1] ^ (2 * block + core)] = out
            rim_ref[places[1] ^ (2 * block + core)] = out[-rim_ref.shape[1] :]


def glu_rows(places, rows, weight_sets, rim):
    count_ep, count_tp = lax.axis_size("ep"), lax.axis_size("tp")
    flat = flat_refs(weight_sets)
    counts = [len(parts) for parts in weight_sets[0][1]]
    channels = flat[0].shape[1] // 2
    length, depth = rows.shape
    return vmem_call(
        functools.partial(glu_body, counts),
        [shape_of((count_tp, length, channels)), shape_of((count_tp, rim, channels))],
        flops=4 * length * depth * channels * count_tp,
        moved=4 * depth * channels * count_tp,
    )(places, by_quarter(rows, count_ep), *flat)


def conv_body(taps, glu_ref, rim_ref, taps_ref, gain_ref, out_ref, held):
    blocks, length, channels = glu_ref.shape
    rim = rim_ref.shape[1]
    span = min(length, 128)
    for block in range(blocks):
        lanes = slice(block * channels, (block + 1) * channels)
        for first in range(0, length, span):
            if first == 0:
                above = rim_ref[block]
            else:
                above = glu_ref[block, first - rim : first, :]
            rows = jnp.concatenate([above, glu_ref[block, first : first + span, :]], axis=0)
            rows = rows.astype(jnp.float32)
            total = jnp.zeros((span, channels), jnp.float32)
            for turn in range(8):
                shifts = [s for s in range(rim - taps + 1, rim + 1) if s % 8 == turn]
                if not shifts:
                    continue
                moved = rows if turn == 0 else jnp.concatenate([rows[turn:], rows[:turn]], axis=0)
                for shift in shifts:
                    tap = shift - (rim - taps + 1)
                    base = shift - turn
                    total = total + taps_ref[tap : tap + 1, lanes] * moved[base : base + span]
            held[first : first + span, lanes] = total
    for first in range(0, length, 32):
        rows = held[first : first + 32, :]
        centred = rows - jnp.mean(rows, axis=-1, keepdims=True)
        spread = jnp.mean(centred * centred, axis=-1, keepdims=True)
        scaled = centred * lax.rsqrt(spread + LAYER_EPSILON) * gain_ref[...]
        out_ref[first : first + 32, :] = (scaled * jax.nn.sigmoid(scaled)).astype(out_ref.dtype)


def project_body(counts, places, rows_ref, gain_ref, *refs):
    out_ref, held = refs[-2], refs[-1]
    width = refs[0].shape[1]
    quarter = refs[0].shape[0] // len(counts)
    squares = jnp.zeros((held.shape[0], 1), jnp.float32)
    for core, (own_ref, pieces) in enumerate(unflat_refs(refs, counts)):
        for block in range(held.shape[1] // width // 2):
            pre = block_products(rows_ref, places, own_ref, pieces, quarter, block)
            squares = squares + jnp.sum(pre * pre, axis=-1, keepdims=True)
            start = pl.multiple_of((places[1] ^ (2 * block + core)) * width, width)
            held[:, pl.ds(start, width)] = pre
    scale = lax.rsqrt(squares / held.shape[1] + RMS_EPSILON)
    out_ref[...] = (held[...] * scale * gain_ref[...]).astype(out_ref.dtype)


def project_rows(places, rows, gain_row, weight_sets):
    count_ep, count_tp = lax.axis_size("ep"), lax.axis_size("tp")
    flat = flat_refs(weight_sets)
    counts = [len(parts) for parts in weight_sets[0][1]]
    length, depth = rows.shape
    width = flat[0].shape[1] * count_tp
    return pl.pallas_call(
        functools.partial(project_body, counts),
        out_shape=jax.ShapeDtypeStruct((length, width), jnp.bfloat16),
        in_specs=[pl.BlockSpec(memory_space=pltpu.SMEM)]
        + [pl.BlockSpec(memory_space=pltpu.VMEM)] * (2 + len(flat)),
        out_specs=pl.BlockSpec(memory_space=pltpu.VMEM),
        scratch_shapes=[pltpu.VMEM((length, width), jnp.float32)],
        cost_estimate=pl.CostEstimate(
            flops=2 * length * depth * width, bytes_accessed=2 * depth * width, transcendentals=0
        ),
        name="project",
    )(places, by_quarter(rows, count_ep), gain_row.reshape(1, -1), *flat)


def vmem_call(body, outs, scratch=(), flops=0, moved=0, smem=1):
    def call(*operands):
        arrays = list(operands[smem:]) + jax.tree.leaves(outs) + [held.inner_aval for held in scratch]
        held_bytes = sum(a.size * a.dtype.itemsize for a in arrays)
        return pl.pallas_call(
            body,
            out_shape=outs,
            in_specs=[pl.BlockSpec(memory_space=pltpu.SMEM)] * smem
            + [pl.BlockSpec(memory_space=pltpu.VMEM)] * (len(operands) - smem),
            out_specs=jax.tree.map(lambda _: pl.BlockSpec(memory_space=pltpu.VMEM), outs),
            scratch_shapes=list(scratch),
            compiler_params=pltpu.CompilerParams(vmem_limit_bytes=held_bytes + SPARE_VMEM),
            cost_estimate=pl.CostEstimate(
                flops=flops, bytes_accessed=moved, transcendentals=0
            ),
        )(*operands)

    return call


def shape_of(dims, kind=jnp.bfloat16):
    return jax.ShapeDtypeStruct(tuple(dims), kind)


def packed(parts):
    def body(*refs):
        for number, ref in enumerate(refs[:-1]):
            refs[-1][number] = ref[...]

    dims = (len(parts),) + parts[0].shape
    return vmem_call(body, shape_of(dims), flops=2 * parts[0].size, smem=0)(*parts)


def token_body(top_count, rows_ref, route_ref, share_ref, out_ref):
    _, width = rows_ref.shape
    out_ref[:, :width] = rows_ref[...]
    share = share_ref[...]
    high = share.astype(jnp.bfloat16).astype(jnp.float32)
    fields = jnp.concatenate([route_ref[...].astype(jnp.float32), high, share - high], axis=0)
    lanes = lax.broadcasted_iota(jnp.int32, (3 * top_count, 128), 1)
    places = lax.broadcasted_iota(jnp.int32, (3 * top_count, 128), 0)
    spread = jnp.where(lanes == places, 1.0, 0.0).astype(jnp.bfloat16)
    extra = lax.dot_general(
        fields.astype(jnp.bfloat16),
        spread,
        (((0,), (0,)), ((), ())),
        preferred_element_type=jnp.float32,
    )
    out_ref[:, width:] = extra.astype(out_ref.dtype)


def pick_body(layout, counts, places, gain_ref, *refs):
    experts, slots, top_count = layout
    parts, (rows_ref, chosen_ref, share_ref) = refs[:-3], refs[-3:]
    width = parts[0].shape[2] - 128
    gain = gain_ref[...]
    at = 0
    for group, count in enumerate(counts):
        block = jnp.concatenate(
            [
                part[number]
                for part in parts[at : at + count]
                for number in range(part.shape[0])
            ],
            axis=0,
        )
        at += count
        length = block.shape[0]
        below = (
            lax.broadcasted_iota(jnp.int32, (length, length), 0)
            > lax.broadcasted_iota(jnp.int32, (length, length), 1)
        ).astype(jnp.bfloat16)
        slot = lax.broadcasted_iota(jnp.int32, (length, slots), 1).astype(jnp.float32)
        lanes = lax.broadcasted_iota(jnp.int32, (length, 128), 1)
        named = block[:, width:].astype(jnp.float32)
        picks, sides = [], []
        for expert in range(experts):
            ident = (places[0] * experts + expert).astype(jnp.float32)
            hit = jnp.zeros((length, 1), jnp.float32)
            share = [jnp.zeros((length, 1), jnp.float32)] * 2
            for column in range(top_count):
                same = named[:, column : column + 1] == ident
                hit = jnp.where(same, 1.0, hit)
                for side in range(2):
                    lane = (side + 1) * top_count + column
                    share[side] = jnp.where(same, named[:, lane : lane + 1], share[side])
            mark = jnp.broadcast_to(hit, (length, 128)).astype(jnp.bfloat16)
            rank = jnp.dot(below, mark, preferred_element_type=jnp.float32)[:, 0:1]
            picks.append(jnp.where((slot == rank) & (hit > 0.0), 1.0, 0.0).astype(jnp.bfloat16))
            sides.append(jnp.where(lanes == 0, share[0], jnp.where(lanes == 1, share[1], 0.0)))
        pick = jnp.concatenate(picks, axis=1)
        chosen_ref[group] = pick
        taken = lax.dot_general(
            pick,
            block[:, :width],
            (((0,), (0,)), ((), ())),
            preferred_element_type=jnp.float32,
        )
        scale = lax.rsqrt(jnp.mean(taken * taken, axis=-1, keepdims=True) + RMS_EPSILON)
        taken = (taken * scale * gain).astype(jnp.bfloat16)
        for expert in range(experts):
            place = slice(group * slots, (group + 1) * slots)
            rows_ref[expert, place, :] = taken[expert * slots : (expert + 1) * slots]
            shares = lax.dot_general(
                picks[expert],
                sides[expert].astype(jnp.bfloat16),
                (((0,), (0,)), ((), ())),
                preferred_element_type=jnp.float32,
            )
            share_ref[expert, place, :] = jnp.broadcast_to(
                shares[:, 0:1] + shares[:, 1:2], (slots, 128)
            )


def picked(places, gain_row, groups, layout):
    experts, slots, _ = layout
    flat = [part for parts in groups for part in parts]
    length = sum(part.shape[0] * part.shape[1] for part in groups[0])
    width = flat[0].shape[2] - 128
    number = len(groups)
    outs = [
        shape_of((experts, number * slots, width)),
        shape_of((number, length, experts * slots)),
        shape_of((experts, number * slots, 128), jnp.float32),
    ]
    body = functools.partial(pick_body, layout, [len(parts) for parts in groups])
    return vmem_call(
        body, outs, flops=2 * number * length * 256 * width, moved=4 * number * length * width
    )(places, gain_row.reshape(1, -1), *flat)


def expert_body(sizes, gate_ref, up_ref, down_ref, *refs):
    count = len(sizes)
    ins, outs, rows = refs[:count], refs[count : 2 * count], refs[2 * count]
    at = 0
    for ref, size in zip(ins, sizes):
        rows[at : at + size] = ref[0]
        at += size
    inner = rows[...]
    gate_pre = jnp.dot(inner, gate_ref[0], preferred_element_type=jnp.float32)
    up_pre = jnp.dot(inner, up_ref[0], preferred_element_type=jnp.float32)
    gate_pre = jnp.minimum(gate_pre, CLAMP_LIMIT)
    up_pre = jnp.clip(up_pre, -CLAMP_LIMIT, CLAMP_LIMIT)
    hidden = ((up_pre + 1.0) * gate_pre * jax.nn.sigmoid(SWISH_ALPHA * gate_pre)).astype(
        jnp.bfloat16
    )
    outcome = jnp.dot(hidden, down_ref[0], preferred_element_type=jnp.float32).astype(jnp.bfloat16)
    at = 0
    for ref, size in zip(outs, sizes):
        ref[0] = outcome[at : at + size]
        at += size


def expert_rows(pieces, gate_proj, up_proj, down_proj):
    experts, width, hidden = gate_proj.shape
    sizes = [piece.shape[1] for piece in pieces]
    row_specs = [pl.BlockSpec((1, size, width), lambda j: (j, 0, 0)) for size in sizes]
    return pl.pallas_call(
        functools.partial(expert_body, sizes),
        grid=(experts,),
        out_shape=[shape_of(piece.shape) for piece in pieces],
        in_specs=[
            pl.BlockSpec((1, width, hidden), lambda j: (j, 0, 0)),
            pl.BlockSpec((1, width, hidden), lambda j: (j, 0, 0)),
            pl.BlockSpec((1, hidden, width), lambda j: (j, 0, 0)),
        ]
        + row_specs,
        out_specs=row_specs,
        scratch_shapes=[pltpu.VMEM((sum(sizes), width), jnp.bfloat16)],
        compiler_params=pltpu.CompilerParams(
            dimension_semantics=("arbitrary",),
            vmem_limit_bytes=12 * width * hidden + 10 * sum(sizes) * width + SPARE_VMEM
            + 20 * sum(sizes) * hidden,
        ),
        cost_estimate=pl.CostEstimate(
            flops=6 * experts * sum(sizes) * width * hidden,
            bytes_accessed=6 * experts * width * hidden,
            transcendentals=0,
        ),
        name="experts",
    )(gate_proj, up_proj, down_proj, *pieces)


def unpick_body(targets, counts, slots, *refs):
    outs = refs[4 * len(counts) :]
    group_at = 0
    for call, count in enumerate(counts):
        own_ref, other_ref, chosen_ref, share_ref = refs[4 * call : 4 * call + 4]
        for group in range(count):
            place = slice(group * slots, (group + 1) * slots)
            rows = jnp.concatenate(
                [
                    (
                        (own_ref[e, place, :].astype(jnp.float32) + other_ref[e, place, :].astype(jnp.float32))
                        * share_ref[e, place, 0:1]
                    ).astype(jnp.bfloat16)
                    for e in range(own_ref.shape[0])
                ],
                axis=0,
            )
            total = jnp.dot(chosen_ref[group], rows, preferred_element_type=jnp.float32)
            total = total.astype(jnp.bfloat16)
            size = total.shape[0] // len(targets[group_at])
            for part, (out, index) in enumerate(targets[group_at]):
                outs[out][index] = total[part * size : (part + 1) * size]
            group_at += 1


def modules(
    mixer_in,
    pre_gain,
    glu_value,
    glu_gate,
    conv_kernel,
    chan_gain,
    out_weight,
    mix_gain,
    expert_in,
    ffn_gain,
    routing,
    route_weight,
    gate_proj,
    up_proj,
    down_proj,
    expert_gain,
):
    count_ep, count_tp = lax.axis_size("ep"), lax.axis_size("tp")
    count_z = count_tp // 2
    ep_index, tp_index = lax.axis_index("ep"), lax.axis_index("tp")
    places = jnp.stack([ep_index, tp_index]).astype(jnp.int32)
    local_experts = gate_proj.shape[0]
    experts = local_experts * count_ep
    token_rows, top_count = routing.shape
    width = expert_in.shape[1]
    capacity = max(2, 3 * token_rows * top_count // (2 * experts))

    tokens = vmem_call(
        functools.partial(token_body, top_count),
        shape_of((token_rows, width + 128)),
        flops=1 << 18,
        smem=0,
    )(expert_in, routing.T, route_weight.T)
    column = packed([tokens] + column_shared(tokens))
    groups = [[column]] + plane_shared(column, 0)

    channels, columns = glu_value.shape[1], out_weight.shape[1]
    glu_own, glu_mine, out_mine = vmem_call(
        weights_body,
        [
            shape_of((width, 2 * channels)),
            shape_of((width // count_ep, 2 * channels)),
            shape_of((out_weight.shape[0] // count_ep, columns)),
        ],
        flops=1 << 20,
    )(places, glu_value, glu_gate, out_weight)
    glu_sets = gathered_blocks(glu_own, glu_mine)
    out_sets = gathered_blocks(out_weight, out_mine)

    slots = -(-capacity * count_z // 16) * 16
    layout = (local_experts, slots, top_count)
    near = picked(places, ffn_gain, groups[:1], layout)
    far = picked(places, ffn_gain, groups[1:], layout)
    pieces = [near[0], far[0]] + [swapped(near[0], 0, 1), swapped(far[0], 0, 1)]
    results = expert_rows(pieces, gate_proj, up_proj, down_proj)
    theirs = [swapped(results[2], 0, 1), swapped(results[3], 0, 1)]

    def added(*parts):
        total = parts[0].astype(jnp.float32)
        for part in parts[1:]:
            total = total + part.astype(jnp.float32)
        return total

    group_rows = count_z * token_rows
    if count_ep == 4:
        half = (2, group_rows // 2, width)
        outs = [shape_of((4,) + half[1:]), shape_of(half), shape_of(half)]
        targets = [[(0, 0), (0, 1)], [(1, 1), (0, 2)], [(0, 3), (2, 1)], [(1, 0), (2, 0)]]
    else:
        outs = [shape_of((count_ep, group_rows, width))]
        targets = [[(0, group)] for group in range(count_ep)]
    chip = vmem_call(
        functools.partial(unpick_body, targets, [1, count_ep - 1], slots),
        outs,
        flops=4 * count_ep * group_rows * 256 * width,
        smem=0,
    )(results[0], theirs[0], near[1], near[2], results[1], theirs[1], far[1], far[2])
    if count_ep == 4:
        first_x = swapped(chip[1], 1, 0)
        first_y = swapped(chip[2], 2, 0)
        passed_x = added(chip[0][2], first_y[0]).astype(jnp.bfloat16)
        passed_y = added(chip[0][3], first_x[0]).astype(jnp.bfloat16)
        last_x = swapped(passed_x, 1, 0)
        last_y = swapped(passed_y, 2, 0)
        summed = jnp.concatenate(
            [added(chip[0][0], first_x[1], last_y), added(chip[0][1], first_y[1], last_x)]
        )
    else:
        summed = added(
            chip[0][0], *[swapped(chip[0][bits], bits, 0) for bits in range(1, count_ep)]
        )
    summed = summed.astype(jnp.bfloat16).reshape(count_z, token_rows, width)
    combined = added(
        summed[0],
        *[swapped(summed[bits], 0, 2 * bits) for bits in range(1, count_z)],
    )
    routed = rms_scale(combined, expert_gain).astype(jnp.bfloat16)

    normed_mix = rms_scale(mixer_in, pre_gain).astype(jnp.bfloat16)
    taps = conv_kernel.shape[0]
    rim = -(-(taps - 1) // 16) * 16
    gated, last_rows = glu_rows(places, normed_mix, glu_sets, rim)
    rim_rows = passed_along(last_rows, ("ep", "tp"), 1)
    length = mixer_in.shape[0]
    activated = vmem_call(
        functools.partial(conv_body, taps),
        shape_of((length, conv_kernel.shape[1])),
        scratch=[pltpu.VMEM((length, conv_kernel.shape[1]), jnp.float32)],
        flops=1 << 32,
        smem=0,
    )(gated, rim_rows, conv_kernel, chan_gain.reshape(1, -1))
    mixed = project_rows(places, activated, mix_gain, out_sets)
    return (mixed, routed)


def solution(mesh):
    in_specs = (
        P(("ep", "tp"), None),
        P(),
        P(None, "tp"),
        P(None, "tp"),
        P(),
        P(),
        P(None, "tp"),
        P(),
        P(("ep", "tp"), None),
        P(),
        P(("ep", "tp"), None),
        P(("ep", "tp"), None),
        P("ep", None, "tp"),
        P("ep", None, "tp"),
        P("ep", "tp", None),
        P(),
    )
    out_specs = (P(("ep", "tp"), None), P(("ep", "tp"), None))
    return jax.shard_map(
        modules, mesh=mesh, in_specs=in_specs, out_specs=out_specs, check_vma=False
    )
```

time: 299 us -> 170 us (0.57)
  waiting for transfers between devices: 221 us -> 88.4 us
  starting transfers between devices: 6.01 us -> 45.1 us
  matrix products: 24.9 us -> 0 us
  Pallas kernels: 0 us -> 23.1 us
  between operations: 14.7 us -> 1.06 us
  blocking collectives: 12.2 us -> 0 us
  other arithmetic: 10.6 us -> 1.97 us
    all_gather x4 -> x0, waiting for transfers between devices: 147 us -> none  [the longest x1 44.1 us: on_device(): lax.all_gather(glu_value, 'tp', axis=1, tiled=True)]
    ppermute x0 -> x44, waiting for transfers between devices: none -> 88.4 us  [swapped(): return lax.ppermute(value, ('ep', 'tp'), pairs)]
    unnamed x6 -> x0, waiting for transfers between devices: 73.5 us -> none
    ppermute x0 -> x44, starting transfers between devices: none -> 43 us  [swapped(): return lax.ppermute(value, ('ep', 'tp'), pairs)]
    dot_general x6 -> x0, matrix products: 24.9 us -> none  [the longest x1 9.8 us: on_device(): jnp.einsum('xecf,efd->xecd', hidden_act, down_proj, preferred_element_typ...]
    pallas_call x0 -> x12, Pallas kernels: none -> 23.1 us  [the longest x10 12.6 us: call(): pl.pallas_call(body, out_shape=outs, in_specs=[pl.BlockSpec(memory_space=...]
    all_to_all x1 -> x0, blocking collectives: 12.2 us -> none  [on_device(): lax.all_to_all(outgoing, 'ep', split_axis=0, concat_axis=0, tiled=True)]
    unnamed x21 -> x56, local copies, waits for them, and re-layouts: 2.76 us -> 10.4 us
  transfers between devices with their start and end apart: 7 -> 45, of which waited for: 5 -> 18; matrix products, arithmetic and copies ran while one was open for 13% -> 1% of each run, Pallas kernels for 0% -> 9%
where the time goes in v1:
time: 170 us
  waiting for transfers between devices  88.4 us (52%)
  starting transfers between devices  45.1 us (27%)
  Pallas kernels  23.1 us (14%)
  local copies, waits for them, and re-layouts  10.6 us (6%)
  other arithmetic  1.97 us (1%)
    ppermute x44, waiting for transfers between devices, swapped(): return lax.ppermute(value, ('ep', 'tp'), pairs)  88.4 us
    ppermute x44, starting transfers between devices, swapped(): return lax.ppermute(value, ('ep', 'tp'), pairs)  43 us
    pallas_call x10, Pallas kernels, call(): pl.pallas_call(body, out_shape=outs, in_specs=[pl.BlockSpec(memory_space=...  12.6 us
    unnamed x56, local copies, waits for them, and re-layouts  10.4 us
    pallas_call x1, Pallas kernels, expert_rows(): pl.pallas_call(functools.partial(expert_body, sizes), grid=(experts,), ou...  5.43 us
    pallas_call x1, Pallas kernels, project_rows(): pl.pallas_call(functools.partial(project_body, counts), out_shape=jax.Sha...  5.05 us
  transfers between devices with their start and end apart: 45, of which 18 were waited for; matrix products, arithmetic and copies ran while one was open for 1% of the time, Pallas kernels for 9%

profile of v1, /device:TPU:0, one launch (start us, length us, event | category | flops | bytes accessed | tf_op | source)
XLA Modules:
  0.0 170.2 jit_solution(10218714730558710263)
XLA Ops:
  0.6 0.9 copy-done.5
  1.5 0.7 copy-done.8
  2.2 0.7 copy-done.9
  3.1 3.1 %collective-permute-start.27 = (bf16[32,2176]{1,0:T(8,128)(2,1)S(1)}, bf16[32,2176]{1,0:T(8,128)(2,1)S(1)}, u32[]{:S(2)}, u32[]{:S(2)}) collective-permute-start(bf16[32,2176]{1,0:T(8,128)(2,1)S(1)} %shard_map.172.refs_0_), channel_id=1, source_target_pairs={{0,2},{1,3},{2,0},{3,1},{4,6},{5,7},{6,4},{7,5},{8,10},{9,11},{10,... | collective-permute-start | bytes 417800 | tf_op jit(solution)/shard_map/ppermute | solution.py:31
  6.1 2.6 %collective-permute-start.28 = (bf16[32,2176]{1,0:T(8,128)(2,1)S(1)}, bf16[32,2176]{1,0:T(8,128)(2,1)S(1)}, u32[]{:S(2)}, u32[]{:S(2)}) collective-permute-start(bf16[32,2176]{1,0:T(8,128)(2,1)S(1)} %shard_map.172.refs_0_), channel_id=1, source_target_pairs={{0,4},{1,5},{2,6},{3,7},{4,0},{5,1},{6,2},{7,3},{8,12},{9,13},{10,... | collective-permute-start | bytes 417800 | tf_op jit(solution)/shard_map/ppermute | solution.py:31
  8.7 2.9 %collective-permute-done.27.refs_1_ = bf16[32,2176]{1,0:T(8,128)(2,1)S(1)} collective-permute-done((bf16[32,2176]{1,0:T(8,128)(2,1)S(1)}, bf16[32,2176]{1,0:T(8,128)(2,1)S(1)}, u32[]{:S(2)}, u32[]{:S(2)}) %collective-permute-start.27) | collective-permute-done | bytes 139296 | tf_op jit(solution)/shard_map/ppermute | solution.py:31
  11.6 7.9 %collective-permute-done.28.refs_2_ = bf16[32,2176]{1,0:T(8,128)(2,1)S(1)} collective-permute-done((bf16[32,2176]{1,0:T(8,128)(2,1)S(1)}, bf16[32,2176]{1,0:T(8,128)(2,1)S(1)}, u32[]{:S(2)}, u32[]{:S(2)}) %collective-permute-start.28) | collective-permute-done | bytes 139296 | tf_op jit(solution)/shard_map/ppermute | solution.py:31
  19.6 1.6 collective-permute-start.30
  21.1 1.5 collective-permute-start.31
  22.7 9.0 %collective-permute-done.30.refs_0_ = bf16[4,32,2176]{2,1,0:T(8,128)(2,1)S(1)} collective-permute-done((bf16[4,32,2176]{2,1,0:T(8,128)(2,1)S(1)}, bf16[4,32,2176]{2,1,0:T(8,128)(2,1)S(1)}, u32[]{:S(2)}, u32[]{:S(2)}) %collective-permute-start.30) | collective-permute-done | bytes 557088 | tf_op jit(solution)/shard_map/ppermute | solution.py:31
  31.6 1.6 collective-permute-start.32
  33.2 1.5 collective-permute-done.31.refs_1_
  35.3 3.5 %collective-permute-done.32.refs_2_ = bf16[2,32,2176]{2,1,0:T(8,128)(2,1)S(1)} collective-permute-done((bf16[2,32,2176]{2,1,0:T(8,128)(2,1)S(1)}, bf16[2,32,2176]{2,1,0:T(8,128)(2,1)S(1)}, u32[]{:S(2)}, u32[]{:S(2)}) %collective-permute-start.32) | collective-permute-done | bytes 278560 | tf_op jit(solution)/shard_map/ppermute | solution.py:31
  38.8 2.6 %collective-permute-done.33.refs_3_ = bf16[2,32,2176]{2,1,0:T(8,128)(2,1)S(1)} collective-permute-done((bf16[2,32,2176]{2,1,0:T(8,128)(2,1)S(1)}, bf16[2,32,2176]{2,1,0:T(8,128)(2,1)S(1)}, u32[]{:S(2)}, u32[]{:S(2)}) %collective-permute-start.33) | collective-permute-done | bytes 278560 | tf_op jit(solution)/shard_map/ppermute | solution.py:31
  41.4 2.7 %shard_map.175 = (bf16[2,144,2048]{2,1,0:T(8,128)(2,1)S(1)}, bf16[3,128,96]{2,1,0:T(8,128)(2,1)S(1)}, f32[2,144,128]{2,1,0:T(8,128)S(1)}) custom-call(s32[2]{0:T(128)S(1)} %pad_add_fusion.places, f32[1,2048]{1,0:T(1,128)S(1)} %bitcast.19, bf16[4,32,2176]{2,1,0:T(8,128)(2,1)S(1)} %collective-permute-done.30.refs_0_, ...), custom_call_target="tpu_custom_call" | custom-call | flops 402653184 | bytes 3145728 | tf_op jit(solution)/shard_map/pallas_call | solution.py:223
  44.2 1.5 shard_map.174
  45.7 0.6 collective-permute-start.34
  46.2 1.3 collective-permute-done.34.refs_2_
  47.6 2.2 %copy-done.10 = bf16[2,2048,512]{2,1,0:T(8,128)(2,1)S(1)} copy-done((bf16[2,2048,512]{2,1,0:T(8,128)(2,1)S(1)}, bf16[2,2048,512]{2,1,0:T(8,128)(2,1)}, u32[]{:S(2)}) %copy-start.10) | copy-done | bytes 4194328
  49.8 2.2 %copy-done.11 = bf16[2,2048,512]{2,1,0:T(8,128)(2,1)S(1)} copy-done((bf16[2,2048,512]{2,1,0:T(8,128)(2,1)S(1)}, bf16[2,2048,512]{2,1,0:T(8,128)(2,1)}, u32[]{:S(2)}) %copy-start.11) | copy-done | bytes 4194328
  52.0 2.2 %copy-done.12 = bf16[2,512,2048]{2,1,0:T(8,128)(2,1)S(1)} copy-done((bf16[2,512,2048]{2,1,0:T(8,128)(2,1)S(1)}, bf16[2,512,2048]{2,1,0:T(8,128)(2,1)}, u32[]{:S(2)}) %copy-start.12) | copy-done | bytes 4194328
  54.2 5.4 %experts.1 = (bf16[2,48,2048]{2,1,0:T(8,128)(2,1)S(1)}, bf16[2,144,2048]{2,1,0:T(8,128)(2,1)S(1)}, bf16[2,48,2048]{2,1,0:T(8,128)(2,1)S(1)}, bf16[2,144,2048]{2,1,0:T(8,128)(2,1)S(1)}) custom-call(bf16[2,2048,512]{2,1,0:T(8,128)(2,1)S(1)} %copy-done.10, bf16[2,2048,512]{2,1,0:T(8,128)(2,1)S(1)} %copy-done.11, bf16[2,512,2048]{2,1,0:T(8,128)(2,1)S(1)} %copy-done.12, ...), custom_call_target="tpu_custom_call" | custom-call | flops 4831838208 | bytes 12582912 | tf_op jit(solution)/shard_map/experts/pallas_call | solution.py:376
  60.1 0.8 shard_map.167
  60.8 2.2 %collective-permute-start = (bf16[512,256]{1,0:T(8,128)(2,1)S(1)}, bf16[512,256]{1,0:T(8,128)(2,1)S(1)}, u32[]{:S(2)}, u32[]{:S(2)}) collective-permute-start(bf16[512,256]{1,0:T(8,128)(2,1)S(1)} %get-tuple-element.21), channel_id=1, source_target_pairs={{0,2},{1,3},{2,0},{3,1},{4,6},{5,7},{6,4},{7,5},{8,10},{9,11},{10,... | collective-permute-start | bytes 786440 | tf_op jit(solution)/shard_map/ppermute | solution.py:31
  63.1 1.1 collective-permute-start.1
  64.2 1.4 collective-permute-start.2
  65.5 1.0 collective-permute-start.14
  66.6 8.7 %collective-permute-done.refs_0_ = bf16[512,256]{1,0:T(8,128)(2,1)S(1)} collective-permute-done((bf16[512,256]{1,0:T(8,128)(2,1)S(1)}, bf16[512,256]{1,0:T(8,128)(2,1)S(1)}, u32[]{:S(2)}, u32[]{:S(2)}) %collective-permute-start) | collective-permute-done | bytes 262176 | tf_op jit(solution)/shard_map/ppermute | solution.py:31
  75.3 9.1 %collective-permute-done.1.refs_1_ = bf16[512,256]{1,0:T(8,128)(2,1)S(1)} collective-permute-done((bf16[512,256]{1,0:T(8,128)(2,1)S(1)}, bf16[512,256]{1,0:T(8,128)(2,1)S(1)}, u32[]{:S(2)}, u32[]{:S(2)}) %collective-permute-start.1) | collective-permute-done | bytes 262176 | tf_op jit(solution)/shard_map/ppermute | solution.py:31
  84.5 1.3 collective-permute-start.3
  85.8 0.5 collective-permute-start.4
  86.3 8.3 %collective-permute-done.15.refs_1_ = bf16[256,256]{1,0:T(8,128)(2,1)S(1)} collective-permute-done((bf16[256,256]{1,0:T(8,128)(2,1)S(1)}, bf16[256,256]{1,0:T(8,128)(2,1)S(1)}, u32[]{:S(2)}, u32[]{:S(2)}) %collective-permute-start.15) | collective-permute-done | bytes 131104 | tf_op jit(solution)/shard_map/ppermute | solution.py:31
  94.6 2.5 %collective-permute-start.16 = (bf16[256,256]{1,0:T(8,128)(2,1)S(1)}, bf16[256,256]{1,0:T(8,128)(2,1)S(1)}, u32[]{:S(2)}, u32[]{:S(2)}) collective-permute-start(bf16[256,256]{1,0:T(8,128)(2,1)S(1)} %get-tuple-element.24), channel_id=1, source_target_pairs={{0,6},{1,7},{2,4},{3,5},{4,2},{5,3},{6,0},{7,1},{8,14},{9,15},{10,... | collective-permute-start | bytes 393224 | tf_op jit(solution)/shard_map/ppermute | solution.py:31
  97.1 4.3 %collective-permute-done.16.refs_2_ = bf16[256,256]{1,0:T(8,128)(2,1)S(1)} collective-permute-done((bf16[256,256]{1,0:T(8,128)(2,1)S(1)}, bf16[256,256]{1,0:T(8,128)(2,1)S(1)}, u32[]{:S(2)}, u32[]{:S(2)}) %collective-permute-start.16) | collective-permute-done | bytes 131104 | tf_op jit(solution)/shard_map/ppermute | solution.py:31
  101.4 1.4 collective-permute-start.17
  102.8 0.5 collective-permute-start.18
  103.3 0.8 shard_map.176
  104.1 8.9 %collective-permute-done.17.refs_2_ = bf16[3,256,256]{2,1,0:T(8,128)(2,1)S(1)} collective-permute-done((bf16[3,256,256]{2,1,0:T(8,128)(2,1)S(1)}, bf16[3,256,256]{2,1,0:T(8,128)(2,1)S(1)}, u32[]{:S(2)}, u32[]{:S(2)}) %collective-permute-start.17) | collective-permute-done | bytes 393248 | tf_op jit(solution)/shard_map/ppermute | solution.py:31
  113.0 1.3 collective-permute-start.38
  114.3 0.5 collective-permute-start.41
  114.9 0.5 collective-permute-start.9
  115.8 1.6 collective-permute-start.5
  117.3 9.1 %collective-permute-done.38 = bf16[2,64,2048]{2,1,0:T(8,128)(2,1)S(1)} collective-permute-done((bf16[2,64,2048]{2,1,0:T(8,128)(2,1)S(1)}, bf16[2,64,2048]{2,1,0:T(8,128)(2,1)S(1)}, u32[]{:S(2)}, u32[]{:S(2)}) %collective-permute-start.38) | collective-permute-done | bytes 524320 | tf_op jit(solution)/shard_map/ppermute | solution.py:31
  126.5 1.3 collective-permute-start.6
  127.8 1.3 collective-permute-done.41
  129.3 6.7 %collective-permute-done.5.refs_4_ = bf16[3,256,256]{2,1,0:T(8,128)(2,1)S(1)} collective-permute-done((bf16[3,256,256]{2,1,0:T(8,128)(2,1)S(1)}, bf16[3,256,256]{2,1,0:T(8,128)(2,1)S(1)}, u32[]{:S(2)}, u32[]{:S(2)}) %collective-permute-start.5) | collective-permute-done | bytes 393248 | tf_op jit(solution)/shard_map/ppermute | solution.py:31
  136.5 1.3 collective-permute-start.39
  137.8 0.9 collective-permute-start.42
  139.6 1.0 collective-permute-start.19
  140.6 3.0 %shard_map.169 = (bf16[8,256,128]{2,1,0:T(8,128)(2,1)S(1)}, bf16[8,32,128]{2,1,0:T(8,128)(2,1)S(1)}) custom-call(s32[2]{0:T(128)S(1)} %pad_add_fusion.places, bf16[256,2048]{1,0:T(8,128)(2,1)S(1)} %fusion.2.rows_ref, bf16[2048,256]{1,0:T(8,128)(2,1)S(1)} %get-tuple-element.20.refs_0_, bf16[3,512,256]{2,1,0:T(8,128)(2,1)S(1)} %shard_map.168.refs_1_, ...), custom_call_target="tpu_custom_call" | custom-call | flops 2147483648 | bytes 8388608 | tf_op jit(solution)/shard_map/pallas_call | solution.py:223
  143.6 2.0 %collective-permute-done.39 = bf16[64,2048]{1,0:T(8,128)(2,1)S(1)} collective-permute-done((bf16[64,2048]{1,0:T(8,128)(2,1)S(1)}, bf16[64,2048]{1,0:T(8,128)(2,1)S(1)}, u32[]{:S(2)}, u32[]{:S(2)}) %collective-permute-start.39) | collective-permute-done | bytes 262176 | tf_op jit(solution)/shard_map/ppermute | solution.py:31
  145.7 1.1 collective-permute-start.20
  147.1 0.6 collective-permute-start.24
  147.7 2.1 %collective-permute-start.13 = (bf16[8,32,128]{2,1,0:T(8,128)(2,1)S(1)}, bf16[8,32,128]{2,1,0:T(8,128)(2,1)S(1)}, u32[]{:S(2)}, u32[]{:S(2)}) collective-permute-start(bf16[8,32,128]{2,1,0:T(8,128)(2,1)S(1)} %get-tuple-element.23), channel_id=1, source_target_pairs={{0,1},{1,2},{2,3},{3,4},{4,5},{5,6},{6,7},{7,8},{8,9},{9,10},{10,1... | collective-permute-start | bytes 196616 | tf_op jit(solution)/shard_map/ppermute | solution.py:21
  149.9 3.8 %collective-permute-start.25 = (bf16[3,128,256]{2,1,0:T(8,128)(2,1)S(1)}, bf16[3,128,256]{2,1,0:T(8,128)(2,1)S(1)}, u32[]{:S(2)}, u32[]{:S(2)}) collective-permute-start(bf16[3,128,256]{2,1,0:T(8,128)(2,1)S(1)} %collective-permute-done.19.refs_4_), channel_id=1, source_target_pairs={{0,1},{1,0},{2,3},{3,2},{4,5},{5,4},{6,7},{7,6},{8,9},{9,8},{10,11... | collective-permute-start | bytes 589832 | tf_op jit(solution)/shard_map/ppermute | solution.py:31
  153.8 0.8 collective-permute-start.44
  154.6 2.4 %collective-permute-start.43 = (bf16[32,2048]{1,0:T(8,128)(2,1)S(1)}, bf16[32,2048]{1,0:T(8,128)(2,1)S(1)}, u32[]{:S(2)}, u32[]{:S(2)}) collective-permute-start(bf16[32,2048]{1,0:T(8,128)(2,1)S(1)} %get-tuple-element.42), channel_id=1, source_target_pairs={{0,4},{1,5},{2,6},{3,7},{4,0},{5,1},{6,2},{7,3},{8,12},{9,13},{10,... | collective-permute-start | bytes 393224 | tf_op jit(solution)/shard_map/ppermute | solution.py:31
  156.9 1.2 collective-permute-start.40
  158.2 3.6 %shard_map.170.rows_ref = bf16[256,1024]{1,0:T(8,128)(2,1)S(1)} custom-call(bf16[8,256,128]{2,1,0:T(8,128)(2,1)S(1)} %get-tuple-element.22.glu_ref, bf16[8,32,128]{2,1,0:T(8,128)(2,1)S(1)} %collective-permute-done.13.rim_ref, f32[31,1024]{1,0:T(8,128)S(1)} %copy-done.13, f32[1,1024]{1,0:T(1,128)S(1)} %bitcast.23), custom_call_target="tpu_custom_call" | custom-call | flops 4294967296 | tf_op jit(solution)/shard_map/pallas_call | solution.py:223
  161.8 0.8 copy-done.2
  162.6 0.7 copy-done.24
  163.4 5.1 %project.1 = bf16[256,2048]{1,0:T(8,128)(2,1)} custom-call(s32[2]{0:T(128)} %copy-done.7, bf16[256,1024]{1,0:T(8,128)(2,1)} %copy-done.2, f32[1,2048]{1,0:T(1,128)} %bitcast.24, bf16[1024,256]{1,0:T(8,128)(2,1)} %refs_0_.1, bf16[3,256,256]{2,1,0:T(8,128)(2,1)} %copy-done.1, bf16[3,256,256]{2,1,0:T(8,128)(2,1)} %copy-done.16, ...), custom_call_target="tpu_custom_call" | custom-call | flops 1073741824 | bytes 4194304 | tf_op jit(solution)/shard_map/project/pallas_call | solution.py:205
  168.4 0.8 collective-permute-done.43
  169.4 0.8 multiply_convert_fusion
  (111 shorter events, 4.0 us)
Async XLA Ops:
  2.9 38.5 %copy-start.6 = (f32[2048]{0:T(1024)S(1)}, f32[2048]{0:T(1024)}, u32[]{:S(2)}) copy-start(f32[2048]{0:T(1024)} %param.25) | copy-start | bytes 24580
  3.1 8.5 %collective-permute-start.27 = (bf16[32,2176]{1,0:T(8,128)(2,1)S(1)}, bf16[32,2176]{1,0:T(8,128)(2,1)S(1)}, u32[]{:S(2)}, u32[]{:S(2)}) collective-permute-start(bf16[32,2176]{1,0:T(8,128)(2,1)S(1)} %shard_map.172.refs_0_), channel_id=1, source_target_pairs={{0,2},{1,3},{2,0},{3,1},{4,6},{5,7},{6,4},{7,5},{8,10},{9,11},{10,... | collective-permute-start | bytes 417800 | tf_op jit(solution)/shard_map/ppermute | solution.py:31
  6.1 13.4 %collective-permute-start.28 = (bf16[32,2176]{1,0:T(8,128)(2,1)S(1)}, bf16[32,2176]{1,0:T(8,128)(2,1)S(1)}, u32[]{:S(2)}, u32[]{:S(2)}) collective-permute-start(bf16[32,2176]{1,0:T(8,128)(2,1)S(1)} %shard_map.172.refs_0_), channel_id=1, source_target_pairs={{0,4},{1,5},{2,6},{3,7},{4,0},{5,1},{6,2},{7,3},{8,12},{9,13},{10,... | collective-permute-start | bytes 417800 | tf_op jit(solution)/shard_map/ppermute | solution.py:31
  8.7 10.8 %collective-permute-start.29 = (bf16[32,2176]{1,0:T(8,128)(2,1)S(1)}, bf16[32,2176]{1,0:T(8,128)(2,1)S(1)}, u32[]{:S(2)}, u32[]{:S(2)}) collective-permute-start(bf16[32,2176]{1,0:T(8,128)(2,1)S(1)} %shard_map.172.refs_0_), channel_id=1, source_target_pairs={{0,6},{1,7},{2,4},{3,5},{4,2},{5,3},{6,0},{7,1},{8,14},{9,15},{10,... | collective-permute-start | bytes 417800 | tf_op jit(solution)/shard_map/ppermute | solution.py:31
  19.6 12.0 %collective-permute-start.30 = (bf16[4,32,2176]{2,1,0:T(8,128)(2,1)S(1)}, bf16[4,32,2176]{2,1,0:T(8,128)(2,1)S(1)}, u32[]{:S(2)}, u32[]{:S(2)}) collective-permute-start(bf16[4,32,2176]{2,1,0:T(8,128)(2,1)S(1)} %shard_map.173.refs_0_), channel_id=1, source_target_pairs={{0,8},{1,9},{2,10},{3,11},{4,12},{5,13},{6,14},{7,15},{8,0},{9,1},... | collective-permute-start | bytes 1671176 | tf_op jit(solution)/shard_map/ppermute | solution.py:31
  21.1 13.6 %collective-permute-start.31 = (bf16[4,32,2176]{2,1,0:T(8,128)(2,1)S(1)}, bf16[4,32,2176]{2,1,0:T(8,128)(2,1)S(1)}, u32[]{:S(2)}, u32[]{:S(2)}) collective-permute-start(bf16[4,32,2176]{2,1,0:T(8,128)(2,1)S(1)} %shard_map.173.refs_0_), channel_id=1, source_target_pairs={{0,16},{1,17},{2,18},{3,19},{4,20},{5,21},{6,22},{7,23},{8,24},{9,... | collective-permute-start | bytes 1671176 | tf_op jit(solution)/shard_map/ppermute | solution.py:31
  31.6 7.2 %collective-permute-start.32 = (bf16[2,32,2176]{2,1,0:T(8,128)(2,1)S(1)}, bf16[2,32,2176]{2,1,0:T(8,128)(2,1)S(1)}, u32[]{:S(2)}, u32[]{:S(2)}) collective-permute-start(bf16[2,32,2176]{2,1,0:T(8,128)(2,1)S(1)} %slice.84), channel_id=1, source_target_pairs={{0,16},{1,17},{2,18},{3,19},{4,20},{5,21},{6,22},{7,23},{8,24},{9,... | collective-permute-start | bytes 835592 | tf_op jit(solution)/shard_map/ppermute | solution.py:31
  34.8 6.6 %collective-permute-start.33 = (bf16[2,32,2176]{2,1,0:T(8,128)(2,1)S(1)}, bf16[2,32,2176]{2,1,0:T(8,128)(2,1)S(1)}, u32[]{:S(2)}, u32[]{:S(2)}) collective-permute-start(bf16[2,32,2176]{2,1,0:T(8,128)(2,1)S(1)} %slice.85), channel_id=1, source_target_pairs={{0,8},{1,9},{2,10},{3,11},{4,12},{5,13},{6,14},{7,15},{8,0},{9,1},... | collective-permute-start | bytes 835592 | tf_op jit(solution)/shard_map/ppermute | solution.py:31
  35.3 105.3 %copy-start.7 = (s32[2]{0:T(128)}, s32[2]{0:T(128)S(1)}, u32[]{:S(2)}) copy-start(s32[2]{0:T(128)S(1)} %pad_add_fusion.places) | copy-start | bytes 28
  44.1 3.5 %collective-permute-start.35 = (bf16[2,144,2048]{2,1,0:T(8,128)(2,1)S(1)}, bf16[2,144,2048]{2,1,0:T(8,128)(2,1)S(1)}, u32[]{:S(2)}, u32[]{:S(2)}) collective-permute-start(bf16[2,144,2048]{2,1,0:T(8,128)(2,1)S(1)} %get-tuple-element.26.refs_1_), channel_id=1, source_target_pairs={{0,1},{1,0},{2,3},{3,2},{4,5},{5,4},{6,7},{7,6},{8,9},{9,8},{10,11... | collective-permute-start | bytes 3538952 | tf_op jit(solution)/shard_map/ppermute | solution.py:31
  45.7 14.4 %copy-start = (bf16[1024,256]{1,0:T(8,128)(2,1)S(1)}, bf16[1024,256]{1,0:T(8,128)(2,1)}, u32[]{:S(2)}) copy-start(bf16[1024,256]{1,0:T(8,128)(2,1)} %refs_0_.1) | copy-start | bytes 1572868
  45.7 14.4 %copy-start.3 = (bf16[2048,128]{1,0:T(8,128)(2,1)S(1)}, bf16[2048,128]{1,0:T(8,128)(2,1)}, u32[]{:S(2)}) copy-start(bf16[2048,128]{1,0:T(8,128)(2,1)} %value_ref.1) | copy-start | bytes 1572868
  45.7 14.4 %copy-start.4 = (bf16[2048,128]{1,0:T(8,128)(2,1)S(1)}, bf16[2048,128]{1,0:T(8,128)(2,1)}, u32[]{:S(2)}) copy-start(bf16[2048,128]{1,0:T(8,128)(2,1)} %gate_ref.2) | copy-start | bytes 1572868
  45.7 1.9 %collective-permute-start.34 = (bf16[2,48,2048]{2,1,0:T(8,128)(2,1)S(1)}, bf16[2,48,2048]{2,1,0:T(8,128)(2,1)S(1)}, u32[]{:S(2)}, u32[]{:S(2)}) collective-permute-start(bf16[2,48,2048]{2,1,0:T(8,128)(2,1)S(1)} %get-tuple-element.25.refs_0_), channel_id=1, source_target_pairs={{0,1},{1,0},{2,3},{3,2},{4,5},{5,4},{6,7},{7,6},{8,9},{9,8},{10,11... | collective-permute-start | bytes 1179656 | tf_op jit(solution)/shard_map/ppermute | solution.py:31
  59.6 43.2 %collective-permute-start.37 = (bf16[2,144,2048]{2,1,0:T(8,128)(2,1)S(1)}, bf16[2,144,2048]{2,1,0:T(8,128)(2,1)S(1)}, u32[]{:S(2)}, u32[]{:S(2)}) collective-permute-start(bf16[2,144,2048]{2,1,0:T(8,128)(2,1)S(1)} %get-tuple-element.32), channel_id=1, source_target_pairs={{0,1},{1,0},{2,3},{3,2},{4,5},{5,4},{6,7},{7,6},{8,9},{9,8},{10,11... | collective-permute-start | bytes 3538952 | tf_op jit(solution)/shard_map/ppermute | solution.py:31
  60.8 14.4 %collective-permute-start = (bf16[512,256]{1,0:T(8,128)(2,1)S(1)}, bf16[512,256]{1,0:T(8,128)(2,1)S(1)}, u32[]{:S(2)}, u32[]{:S(2)}) collective-permute-start(bf16[512,256]{1,0:T(8,128)(2,1)S(1)} %get-tuple-element.21), channel_id=1, source_target_pairs={{0,2},{1,3},{2,0},{3,1},{4,6},{5,7},{6,4},{7,5},{8,10},{9,11},{10,... | collective-permute-start | bytes 786440 | tf_op jit(solution)/shard_map/ppermute | solution.py:31
  63.1 21.3 %collective-permute-start.1 = (bf16[512,256]{1,0:T(8,128)(2,1)S(1)}, bf16[512,256]{1,0:T(8,128)(2,1)S(1)}, u32[]{:S(2)}, u32[]{:S(2)}) collective-permute-start(bf16[512,256]{1,0:T(8,128)(2,1)S(1)} %get-tuple-element.21), channel_id=1, source_target_pairs={{0,4},{1,5},{2,6},{3,7},{4,0},{5,1},{6,2},{7,3},{8,12},{9,13},{10,... | collective-permute-start | bytes 786440 | tf_op jit(solution)/shard_map/ppermute | solution.py:31
  64.2 20.2 %collective-permute-start.2 = (bf16[512,256]{1,0:T(8,128)(2,1)S(1)}, bf16[512,256]{1,0:T(8,128)(2,1)S(1)}, u32[]{:S(2)}, u32[]{:S(2)}) collective-permute-start(bf16[512,256]{1,0:T(8,128)(2,1)S(1)} %get-tuple-element.21), channel_id=1, source_target_pairs={{0,6},{1,7},{2,4},{3,5},{4,2},{5,3},{6,0},{7,1},{8,14},{9,15},{10,... | collective-permute-start | bytes 786440 | tf_op jit(solution)/shard_map/ppermute | solution.py:31
  65.5 20.2 %collective-permute-start.14 = (bf16[256,256]{1,0:T(8,128)(2,1)S(1)}, bf16[256,256]{1,0:T(8,128)(2,1)S(1)}, u32[]{:S(2)}, u32[]{:S(2)}) collective-permute-start(bf16[256,256]{1,0:T(8,128)(2,1)S(1)} %get-tuple-element.24), channel_id=1, source_target_pairs={{0,2},{1,3},{2,0},{3,1},{4,6},{5,7},{6,4},{7,5},{8,10},{9,11},{10,... | collective-permute-start | bytes 393224 | tf_op jit(solution)/shard_map/ppermute | solution.py:31
  75.3 19.3 %collective-permute-start.15 = (bf16[256,256]{1,0:T(8,128)(2,1)S(1)}, bf16[256,256]{1,0:T(8,128)(2,1)S(1)}, u32[]{:S(2)}, u32[]{:S(2)}) collective-permute-start(bf16[256,256]{1,0:T(8,128)(2,1)S(1)} %get-tuple-element.24), channel_id=1, source_target_pairs={{0,4},{1,5},{2,6},{3,7},{4,0},{5,1},{6,2},{7,3},{8,12},{9,13},{10,... | collective-permute-start | bytes 393224 | tf_op jit(solution)/shard_map/ppermute | solution.py:31
  84.4 17.0 %collective-permute-start.36 = (bf16[2,48,2048]{2,1,0:T(8,128)(2,1)S(1)}, bf16[2,48,2048]{2,1,0:T(8,128)(2,1)S(1)}, u32[]{:S(2)}, u32[]{:S(2)}) collective-permute-start(bf16[2,48,2048]{2,1,0:T(8,128)(2,1)S(1)} %get-tuple-element.28), channel_id=1, source_target_pairs={{0,1},{1,0},{2,3},{3,2},{4,5},{5,4},{6,7},{7,6},{8,9},{9,8},{10,11... | collective-permute-start | bytes 1179656 | tf_op jit(solution)/shard_map/ppermute | solution.py:31
  84.5 30.4 %collective-permute-start.3 = (bf16[3,512,256]{2,1,0:T(8,128)(2,1)S(1)}, bf16[3,512,256]{2,1,0:T(8,128)(2,1)S(1)}, u32[]{:S(2)}, u32[]{:S(2)}) collective-permute-start(bf16[3,512,256]{2,1,0:T(8,128)(2,1)S(1)} %shard_map.168.refs_1_), channel_id=1, source_target_pairs={{0,8},{1,9},{2,10},{3,11},{4,12},{5,13},{6,14},{7,15},{8,0},{9,1},... | collective-permute-start | bytes 2359304 | tf_op jit(solution)/shard_map/ppermute | solution.py:31
  85.8 29.1 %collective-permute-start.4 = (bf16[3,512,256]{2,1,0:T(8,128)(2,1)S(1)}, bf16[3,512,256]{2,1,0:T(8,128)(2,1)S(1)}, u32[]{:S(2)}, u32[]{:S(2)}) collective-permute-start(bf16[3,512,256]{2,1,0:T(8,128)(2,1)S(1)} %shard_map.168.refs_1_), channel_id=1, source_target_pairs={{0,16},{1,17},{2,18},{3,19},{4,20},{5,21},{6,22},{7,23},{8,24},{9,... | collective-permute-start | bytes 2359304 | tf_op jit(solution)/shard_map/ppermute | solution.py:31
  94.6 6.8 %collective-permute-start.16 = (bf16[256,256]{1,0:T(8,128)(2,1)S(1)}, bf16[256,256]{1,0:T(8,128)(2,1)S(1)}, u32[]{:S(2)}, u32[]{:S(2)}) collective-permute-start(bf16[256,256]{1,0:T(8,128)(2,1)S(1)} %get-tuple-element.24), channel_id=1, source_target_pairs={{0,6},{1,7},{2,4},{3,5},{4,2},{5,3},{6,0},{7,1},{8,14},{9,15},{10,... | collective-permute-start | bytes 393224 | tf_op jit(solution)/shard_map/ppermute | solution.py:31
  101.3 14.4 %collective-permute-start.7 = (bf16[2048,256]{1,0:T(8,128)(2,1)S(1)}, bf16[2048,256]{1,0:T(8,128)(2,1)S(1)}, u32[]{:S(2)}, u32[]{:S(2)}) collective-permute-start(bf16[2048,256]{1,0:T(8,128)(2,1)S(1)} %get-tuple-element.20.refs_0_), channel_id=1, source_target_pairs={{0,1},{1,0},{2,3},{3,2},{4,5},{5,4},{6,7},{7,6},{8,9},{9,8},{10,11... | collective-permute-start | bytes 3145736 | tf_op jit(solution)/shard_map/ppermute | solution.py:31
  101.4 37.8 %copy-start.1 = (bf16[3,256,256]{2,1,0:T(8,128)(2,1)}, bf16[3,256,256]{2,1,0:T(8,128)(2,1)S(1)}, u32[]{:S(2)}) copy-start(bf16[3,256,256]{2,1,0:T(8,128)(2,1)S(1)} %shard_map.171.refs_1_) | copy-start | bytes 1179652
  101.4 14.0 %copy-start.15 = (bf16[256,2048]{1,0:T(8,128)(2,1)S(1)}, bf16[256,2048]{1,0:T(8,128)(2,1)}, u32[]{:S(2)}) copy-start(bf16[256,2048]{1,0:T(8,128)(2,1)} %param.16) | copy-start | bytes 3145732
  101.4 11.6 %collective-permute-start.17 = (bf16[3,256,256]{2,1,0:T(8,128)(2,1)S(1)}, bf16[3,256,256]{2,1,0:T(8,128)(2,1)S(1)}, u32[]{:S(2)}, u32[]{:S(2)}) collective-permute-start(bf16[3,256,256]{2,1,0:T(8,128)(2,1)S(1)} %shard_map.171.refs_1_), channel_id=1, source_target_pairs={{0,8},{1,9},{2,10},{3,11},{4,12},{5,13},{6,14},{7,15},{8,0},{9,1},... | collective-permute-start | bytes 1179656 | tf_op jit(solution)/shard_map/ppermute | solution.py:31
  102.8 11.5 %collective-permute-start.18 = (bf16[3,256,256]{2,1,0:T(8,128)(2,1)S(1)}, bf16[3,256,256]{2,1,0:T(8,128)(2,1)S(1)}, u32[]{:S(2)}, u32[]{:S(2)}) collective-permute-start(bf16[3,256,256]{2,1,0:T(8,128)(2,1)S(1)} %shard_map.171.refs_1_), channel_id=1, source_target_pairs={{0,16},{1,17},{2,18},{3,19},{4,20},{5,21},{6,22},{7,23},{8,24},{9,... | collective-permute-start | bytes 1179656 | tf_op jit(solution)/shard_map/ppermute | solution.py:31
  113.0 33.8 %copy-start.16 = (bf16[3,256,256]{2,1,0:T(8,128)(2,1)}, bf16[3,256,256]{2,1,0:T(8,128)(2,1)S(1)}, u32[]{:S(2)}) copy-start(bf16[3,256,256]{2,1,0:T(8,128)(2,1)S(1)} %collective-permute-done.17.refs_2_) | copy-start | bytes 1179652
  113.0 13.5 %collective-permute-start.38 = (bf16[2,64,2048]{2,1,0:T(8,128)(2,1)S(1)}, bf16[2,64,2048]{2,1,0:T(8,128)(2,1)S(1)}, u32[]{:S(2)}, u32[]{:S(2)}) collective-permute-start(bf16[2,64,2048]{2,1,0:T(8,128)(2,1)S(1)} %get-tuple-element.36), channel_id=1, source_target_pairs={{0,8},{1,9},{2,10},{3,11},{4,12},{5,13},{6,14},{7,15},{8,0},{9,1},... | collective-permute-start | bytes 1572872 | tf_op jit(solution)/shard_map/ppermute | solution.py:31
  114.3 32.7 %copy-start.17 = (bf16[3,256,256]{2,1,0:T(8,128)(2,1)}, bf16[3,256,256]{2,1,0:T(8,128)(2,1)S(1)}, u32[]{:S(2)}) copy-start(bf16[3,256,256]{2,1,0:T(8,128)(2,1)S(1)} %collective-permute-done.18.refs_3_) | copy-start | bytes 1179652
  114.3 24.3 %copy-start.26 = (f32[2048]{0:T(1024)S(1)}, f32[2048]{0:T(1024)}, u32[]{:S(2)}) copy-start(f32[2048]{0:T(1024)} %param.17) | copy-start | bytes 24580
  114.3 14.8 %collective-permute-start.41 = (bf16[2,64,2048]{2,1,0:T(8,128)(2,1)S(1)}, bf16[2,64,2048]{2,1,0:T(8,128)(2,1)S(1)}, u32[]{:S(2)}, u32[]{:S(2)}) collective-permute-start(bf16[2,64,2048]{2,1,0:T(8,128)(2,1)S(1)} %get-tuple-element.37), channel_id=1, source_target_pairs={{0,16},{1,17},{2,18},{3,19},{4,20},{5,21},{6,22},{7,23},{8,24},{9,... | collective-permute-start | bytes 1572872 | tf_op jit(solution)/shard_map/ppermute | solution.py:31
  114.9 21.6 %collective-permute-start.8 = (bf16[3,512,256]{2,1,0:T(8,128)(2,1)S(1)}, bf16[3,512,256]{2,1,0:T(8,128)(2,1)S(1)}, u32[]{:S(2)}, u32[]{:S(2)}) collective-permute-start(bf16[3,512,256]{2,1,0:T(8,128)(2,1)S(1)} %shard_map.168.refs_1_), channel_id=1, source_target_pairs={{0,1},{1,0},{2,3},{3,2},{4,5},{5,4},{6,7},{7,6},{8,9},{9,8},{10,11... | collective-permute-start | bytes 2359304 | tf_op jit(solution)/shard_map/ppermute | solution.py:31
  114.9 22.9 %collective-permute-start.9 = (bf16[3,512,256]{2,1,0:T(8,128)(2,1)S(1)}, bf16[3,512,256]{2,1,0:T(8,128)(2,1)S(1)}, u32[]{:S(2)}, u32[]{:S(2)}) collective-permute-start(bf16[3,512,256]{2,1,0:T(8,128)(2,1)S(1)} %collective-permute-done.3.refs_2_), channel_id=1, source_target_pairs={{0,1},{1,0},{2,3},{3,2},{4,5},{5,4},{6,7},{7,6},{8,9},{9,8},{10,11... | collective-permute-start | bytes 2359304 | tf_op jit(solution)/shard_map/ppermute | solution.py:31
  115.8 20.2 %collective-permute-start.5 = (bf16[3,256,256]{2,1,0:T(8,128)(2,1)S(1)}, bf16[3,256,256]{2,1,0:T(8,128)(2,1)S(1)}, u32[]{:S(2)}, u32[]{:S(2)}) collective-permute-start(bf16[3,256,256]{2,1,0:T(8,128)(2,1)S(1)} %slice.80), channel_id=1, source_target_pairs={{0,16},{1,17},{2,18},{3,19},{4,20},{5,21},{6,22},{7,23},{8,24},{9,... | collective-permute-start | bytes 1179656 | tf_op jit(solution)/shard_map/ppermute | solution.py:31
  126.5 9.8 %collective-permute-start.6 = (bf16[3,256,256]{2,1,0:T(8,128)(2,1)S(1)}, bf16[3,256,256]{2,1,0:T(8,128)(2,1)S(1)}, u32[]{:S(2)}, u32[]{:S(2)}) collective-permute-start(bf16[3,256,256]{2,1,0:T(8,128)(2,1)S(1)} %slice.81), channel_id=1, source_target_pairs={{0,8},{1,9},{2,10},{3,11},{4,12},{5,13},{6,14},{7,15},{8,0},{9,1},... | collective-permute-start | bytes 1179656 | tf_op jit(solution)/shard_map/ppermute | solution.py:31
  129.1 9.9 %collective-permute-start.10 = (bf16[3,512,256]{2,1,0:T(8,128)(2,1)S(1)}, bf16[3,512,256]{2,1,0:T(8,128)(2,1)S(1)}, u32[]{:S(2)}, u32[]{:S(2)}) collective-permute-start(bf16[3,512,256]{2,1,0:T(8,128)(2,1)S(1)} %collective-permute-done.4.refs_3_), channel_id=1, source_target_pairs={{0,1},{1,0},{2,3},{3,2},{4,5},{5,4},{6,7},{7,6},{8,9},{9,8},{10,11... | collective-permute-start | bytes 2359304 | tf_op jit(solution)/shard_map/ppermute | solution.py:31
  136.0 3.2 %collective-permute-start.11 = (bf16[3,256,256]{2,1,0:T(8,128)(2,1)S(1)}, bf16[3,256,256]{2,1,0:T(8,128)(2,1)S(1)}, u32[]{:S(2)}, u32[]{:S(2)}) collective-permute-start(bf16[3,256,256]{2,1,0:T(8,128)(2,1)S(1)} %collective-permute-done.5.refs_4_), channel_id=1, source_target_pairs={{0,1},{1,0},{2,3},{3,2},{4,5},{5,4},{6,7},{7,6},{8,9},{9,8},{10,11... | collective-permute-start | bytes 1179656 | tf_op jit(solution)/shard_map/ppermute | solution.py:31
  136.3 3.4 %collective-permute-start.12 = (bf16[3,256,256]{2,1,0:T(8,128)(2,1)S(1)}, bf16[3,256,256]{2,1,0:T(8,128)(2,1)S(1)}, u32[]{:S(2)}, u32[]{:S(2)}) collective-permute-start(bf16[3,256,256]{2,1,0:T(8,128)(2,1)S(1)} %collective-permute-done.6.refs_5_), channel_id=1, source_target_pairs={{0,1},{1,0},{2,3},{3,2},{4,5},{5,4},{6,7},{7,6},{8,9},{9,8},{10,11... | collective-permute-start | bytes 1179656 | tf_op jit(solution)/shard_map/ppermute | solution.py:31
  136.5 9.2 %collective-permute-start.39 = (bf16[64,2048]{1,0:T(8,128)(2,1)S(1)}, bf16[64,2048]{1,0:T(8,128)(2,1)S(1)}, u32[]{:S(2)}, u32[]{:S(2)}) collective-permute-start(bf16[64,2048]{1,0:T(8,128)(2,1)S(1)} %get-tuple-element.40), channel_id=1, source_target_pairs={{0,16},{1,17},{2,18},{3,19},{4,20},{5,21},{6,22},{7,23},{8,24},{9,... | collective-permute-start | bytes 786440 | tf_op jit(solution)/shard_map/ppermute | solution.py:31
  137.8 9.0 %collective-permute-start.42 = (bf16[64,2048]{1,0:T(8,128)(2,1)S(1)}, bf16[64,2048]{1,0:T(8,128)(2,1)S(1)}, u32[]{:S(2)}, u32[]{:S(2)}) collective-permute-start(bf16[64,2048]{1,0:T(8,128)(2,1)S(1)} %get-tuple-element.41), channel_id=1, source_target_pairs={{0,8},{1,9},{2,10},{3,11},{4,12},{5,13},{6,14},{7,15},{8,0},{9,1},... | collective-permute-start | bytes 786440 | tf_op jit(solution)/shard_map/ppermute | solution.py:31
  139.1 8.0 %collective-permute-start.21 = (bf16[1024,256]{1,0:T(8,128)(2,1)S(1)}, bf16[1024,256]{1,0:T(8,128)(2,1)S(1)}, u32[]{:S(2)}, u32[]{:S(2)}) collective-permute-start(bf16[1024,256]{1,0:T(8,128)(2,1)S(1)} %copy-done), channel_id=1, source_target_pairs={{0,1},{1,0},{2,3},{3,2},{4,5},{5,4},{6,7},{7,6},{8,9},{9,8},{10,11... | collective-permute-start | bytes 1572872 | tf_op jit(solution)/shard_map/ppermute | solution.py:31
  139.2 8.5 %collective-permute-start.22 = (bf16[3,256,256]{2,1,0:T(8,128)(2,1)S(1)}, bf16[3,256,256]{2,1,0:T(8,128)(2,1)S(1)}, u32[]{:S(2)}, u32[]{:S(2)}) collective-permute-start(bf16[3,256,256]{2,1,0:T(8,128)(2,1)S(1)} %shard_map.171.refs_1_), channel_id=1, source_target_pairs={{0,1},{1,0},{2,3},{3,2},{4,5},{5,4},{6,7},{7,6},{8,9},{9,8},{10,11... | collective-permute-start | bytes 1179656 | tf_op jit(solution)/shard_map/ppermute | solution.py:31
  139.6 10.2 %collective-permute-start.19 = (bf16[3,128,256]{2,1,0:T(8,128)(2,1)S(1)}, bf16[3,128,256]{2,1,0:T(8,128)(2,1)S(1)}, u32[]{:S(2)}, u32[]{:S(2)}) collective-permute-start(bf16[3,128,256]{2,1,0:T(8,128)(2,1)S(1)} %slice.82), channel_id=1, source_target_pairs={{0,16},{1,17},{2,18},{3,19},{4,20},{5,21},{6,22},{7,23},{8,24},{9,... | collective-permute-start | bytes 589832 | tf_op jit(solution)/shard_map/ppermute | solution.py:31
  143.6 14.5 %copy-start.13 = (f32[31,1024]{1,0:T(8,128)S(1)}, f32[31,1024]{1,0:T(8,128)}, u32[]{:S(2)}) copy-start(f32[31,1024]{1,0:T(8,128)} %taps_ref.1) | copy-start | bytes 380932
  143.6 14.5 %copy-start.14 = (f32[1024]{0:T(1024)S(1)}, f32[1024]{0:T(1024)}, u32[]{:S(2)}) copy-start(f32[1024]{0:T(1024)} %param.21) | copy-start | bytes 12292
  145.7 8.0 %collective-permute-start.20 = (bf16[3,128,256]{2,1,0:T(8,128)(2,1)S(1)}, bf16[3,128,256]{2,1,0:T(8,128)(2,1)S(1)}, u32[]{:S(2)}, u32[]{:S(2)}) collective-permute-start(bf16[3,128,256]{2,1,0:T(8,128)(2,1)S(1)} %slice.83), channel_id=1, source_target_pairs={{0,8},{1,9},{2,10},{3,11},{4,12},{5,13},{6,14},{7,15},{8,0},{9,1},... | collective-permute-start | bytes 589832 | tf_op jit(solution)/shard_map/ppermute | solution.py:31
  146.8 6.9 %collective-permute-start.23 = (bf16[3,256,256]{2,1,0:T(8,128)(2,1)S(1)}, bf16[3,256,256]{2,1,0:T(8,128)(2,1)S(1)}, u32[]{:S(2)}, u32[]{:S(2)}) collective-permute-start(bf16[3,256,256]{2,1,0:T(8,128)(2,1)S(1)} %collective-permute-done.17.refs_2_), channel_id=1, source_target_pairs={{0,1},{1,0},{2,3},{3,2},{4,5},{5,4},{6,7},{7,6},{8,9},{9,8},{10,11... | collective-permute-start | bytes 1179656 | tf_op jit(solution)/shard_map/ppermute | solution.py:31
  147.1 14.7 %copy-start.18 = (bf16[1024,256]{1,0:T(8,128)(2,1)}, bf16[1024,256]{1,0:T(8,128)(2,1)S(1)}, u32[]{:S(2)}) copy-start(bf16[1024,256]{1,0:T(8,128)(2,1)S(1)} %collective-permute-done.21.refs_6_) | copy-start | bytes 1572868
  147.1 7.5 %collective-permute-start.24 = (bf16[3,256,256]{2,1,0:T(8,128)(2,1)S(1)}, bf16[3,256,256]{2,1,0:T(8,128)(2,1)S(1)}, u32[]{:S(2)}, u32[]{:S(2)}) collective-permute-start(bf16[3,256,256]{2,1,0:T(8,128)(2,1)S(1)} %collective-permute-done.18.refs_3_), channel_id=1, source_target_pairs={{0,1},{1,0},{2,3},{3,2},{4,5},{5,4},{6,7},{7,6},{8,9},{9,8},{10,11... | collective-permute-start | bytes 1179656 | tf_op jit(solution)/shard_map/ppermute | solution.py:31
  147.7 14.1 %copy-start.19 = (bf16[3,256,256]{2,1,0:T(8,128)(2,1)}, bf16[3,256,256]{2,1,0:T(8,128)(2,1)S(1)}, u32[]{:S(2)}) copy-start(bf16[3,256,256]{2,1,0:T(8,128)(2,1)S(1)} %collective-permute-done.22.refs_7_) | copy-start | bytes 1179652
  147.7 9.2 %collective-permute-start.13 = (bf16[8,32,128]{2,1,0:T(8,128)(2,1)S(1)}, bf16[8,32,128]{2,1,0:T(8,128)(2,1)S(1)}, u32[]{:S(2)}, u32[]{:S(2)}) collective-permute-start(bf16[8,32,128]{2,1,0:T(8,128)(2,1)S(1)} %get-tuple-element.23), channel_id=1, source_target_pairs={{0,1},{1,2},{2,3},{3,4},{4,5},{5,6},{6,7},{7,8},{8,9},{9,10},{10,1... | collective-permute-start | bytes 196616 | tf_op jit(solution)/shard_map/ppermute | solution.py:21
  149.9 11.9 %copy-start.22 = (bf16[3,128,256]{2,1,0:T(8,128)(2,1)}, bf16[3,128,256]{2,1,0:T(8,128)(2,1)S(1)}, u32[]{:S(2)}) copy-start(bf16[3,128,256]{2,1,0:T(8,128)(2,1)S(1)} %collective-permute-done.19.refs_4_) | copy-start | bytes 589828
  149.9 12.8 %collective-permute-start.25 = (bf16[3,128,256]{2,1,0:T(8,128)(2,1)S(1)}, bf16[3,128,256]{2,1,0:T(8,128)(2,1)S(1)}, u32[]{:S(2)}, u32[]{:S(2)}) collective-permute-start(bf16[3,128,256]{2,1,0:T(8,128)(2,1)S(1)} %collective-permute-done.19.refs_4_), channel_id=1, source_target_pairs={{0,1},{1,0},{2,3},{3,2},{4,5},{5,4},{6,7},{7,6},{8,9},{9,8},{10,11... | collective-permute-start | bytes 589832 | tf_op jit(solution)/shard_map/ppermute | solution.py:31
  153.7 8.1 %copy-start.23 = (bf16[3,128,256]{2,1,0:T(8,128)(2,1)}, bf16[3,128,256]{2,1,0:T(8,128)(2,1)S(1)}, u32[]{:S(2)}) copy-start(bf16[3,128,256]{2,1,0:T(8,128)(2,1)S(1)} %collective-permute-done.20.refs_5_) | copy-start | bytes 589828
  153.7 9.0 %collective-permute-start.26 = (bf16[3,128,256]{2,1,0:T(8,128)(2,1)S(1)}, bf16[3,128,256]{2,1,0:T(8,128)(2,1)S(1)}, u32[]{:S(2)}, u32[]{:S(2)}) collective-permute-start(bf16[3,128,256]{2,1,0:T(8,128)(2,1)S(1)} %collective-permute-done.20.refs_5_), channel_id=1, source_target_pairs={{0,1},{1,0},{2,3},{3,2},{4,5},{5,4},{6,7},{7,6},{8,9},{9,8},{10,11... | collective-permute-start | bytes 589832 | tf_op jit(solution)/shard_map/ppermute | solution.py:31
  153.8 8.0 %copy-start.20 = (bf16[3,256,256]{2,1,0:T(8,128)(2,1)}, bf16[3,256,256]{2,1,0:T(8,128)(2,1)S(1)}, u32[]{:S(2)}) copy-start(bf16[3,256,256]{2,1,0:T(8,128)(2,1)S(1)} %collective-permute-done.23.refs_8_) | copy-start | bytes 1179652
  153.8 14.7 %collective-permute-start.44 = (bf16[32,2048]{1,0:T(8,128)(2,1)S(1)}, bf16[32,2048]{1,0:T(8,128)(2,1)S(1)}, u32[]{:S(2)}, u32[]{:S(2)}) collective-permute-start(bf16[32,2048]{1,0:T(8,128)(2,1)S(1)} %get-tuple-element.43), channel_id=1, source_target_pairs={{0,6},{1,7},{2,4},{3,5},{4,2},{5,3},{6,0},{7,1},{8,14},{9,15},{10,... | collective-permute-start | bytes 393224 | tf_op jit(solution)/shard_map/ppermute | solution.py:31
  154.6 7.2 %copy-start.21 = (bf16[3,256,256]{2,1,0:T(8,128)(2,1)}, bf16[3,256,256]{2,1,0:T(8,128)(2,1)S(1)}, u32[]{:S(2)}) copy-start(bf16[3,256,256]{2,1,0:T(8,128)(2,1)S(1)} %collective-permute-done.24.refs_9_) | copy-start | bytes 1179652
  154.6 14.7 %collective-permute-start.43 = (bf16[32,2048]{1,0:T(8,128)(2,1)S(1)}, bf16[32,2048]{1,0:T(8,128)(2,1)S(1)}, u32[]{:S(2)}, u32[]{:S(2)}) collective-permute-start(bf16[32,2048]{1,0:T(8,128)(2,1)S(1)} %get-tuple-element.42), channel_id=1, source_target_pairs={{0,4},{1,5},{2,6},{3,7},{4,0},{5,1},{6,2},{7,3},{8,12},{9,13},{10,... | collective-permute-start | bytes 393224 | tf_op jit(solution)/shard_map/ppermute | solution.py:31
  156.9 12.3 %collective-permute-start.40 = (bf16[32,2048]{1,0:T(8,128)(2,1)S(1)}, bf16[32,2048]{1,0:T(8,128)(2,1)S(1)}, u32[]{:S(2)}, u32[]{:S(2)}) collective-permute-start(bf16[32,2048]{1,0:T(8,128)(2,1)S(1)} %slice.89), channel_id=1, source_target_pairs={{0,2},{1,3},{2,0},{3,1},{4,6},{5,7},{6,4},{7,5},{8,10},{9,11},{10,... | collective-permute-start | bytes 393224 | tf_op jit(solution)/shard_map/ppermute | solution.py:31
  163.4 6.1 %copy-start.27 = (f32[2048]{0:T(1024)S(1)}, f32[2048]{0:T(1024)}, u32[]{:S(2)}) copy-start(f32[2048]{0:T(1024)} %param.31) | copy-start | bytes 24580
  (9 other events, 11.1 us)
